TPU v7x, 32 devices: a whole 2x2x4 slice. The times are simulated.
32 devices in a mesh: sp: 8 (over z, x), tp: 4 (over y, core).
Axes of the slice: x: 2, y: 2, z: 4, core: 2. Of those that a mesh axis runs over, the one named last changes fastest.
Arguments:
- query_one: bfloat16 [2048, 1024], P('sp', 'tp'), may hold values from -6 to 6
- key_one: bfloat16 [2048, 1024], P('sp', 'tp'), may hold values from -6 to 6
- value_one: bfloat16 [2048, 2048], P('sp', 'tp'), may hold values from -6 to 6
- gate_one: bfloat16 [2048, 2048], P('sp', 'tp'), may hold values from -6 to 6
- decay_one: float32 [2, 2048, 1024], P(None, 'sp', 'tp')
- query_two: bfloat16 [2048, 2048], P('sp', 'tp'), may hold values from -6 to 6
- key_two: bfloat16 [2048, 2048], P('sp', 'tp'), may hold values from -6 to 6
- value_two: bfloat16 [2048, 2048], P('sp', 'tp'), may hold values from -6 to 6
- gate_two: bfloat16 [2048, 2048], P('sp', 'tp'), may hold values from -6 to 6
- decay_two: float32 [2, 2048, 2048], P(None, 'sp', 'tp')
- head_gain: float32 [128], replicated, may hold values from 0.1 to 1.9
- proj_one: bfloat16 [2048, 2048], P('tp'), may hold values from -0.09375 to 0.09375
- proj_two: bfloat16 [2048, 2048], P('tp'), may hold values from -0.09375 to 0.09375
- stream: bfloat16 [2048, 2048], P('sp'), may hold values from -6 to 6
- gain_mix: float32 [2048], replicated, may hold values from 0.1 to 1.9
- gain_moe: float32 [2048], replicated, may hold values from 0.1 to 1.9
- routes: int32 [2048, 2], P('sp'), may hold values from 0 to 7, all different within a row; in each aligned block of 256 rows (0 to 255, 256 to 511, ...) at most 96 rows name the same one
- affinity: float32 [2048, 2], P('sp'), may hold values from 0.1 to 1
- expert_gate: bfloat16 [8, 2048, 2048], P('sp', None, 'tp'), may hold values from -0.125 to 0.125
- expert_up: bfloat16 [8, 2048, 2048], P('sp', None, 'tp'), may hold values from -0.125 to 0.125
- expert_down: bfloat16 [8, 2048, 2048], P('sp', 'tp'), may hold values from -0.125 to 0.125
Outputs:
- output: bfloat16 [2048, 2048], P(('sp', 'tp'))
Inputs may be any that keep to these rules, and one draw needn't show every extreme that they name: `routes`: in the 256 rows of one index of sp no expert is named more than 96 times, a bound that some block reaches there in every draw; a row names 2 different experts.
All inputs are finite; a program needn't handle non-finite values.
Results may differ from a plain program's by a relative error of at most 0.017.
Values may be sent and summed in bfloat16 or wider, within the bound.
A program may use at most 64 MiB of HBM per device.

v0:
```python
import jax
import jax.numpy as jnp
from jax import lax
from jax.sharding import PartitionSpec as P

DK_A = 64
DK_B = 128
BLK = 64


normalizer_sharpness = 16.0
highest = lax.Precision.HIGHEST


def carried_in(value, axis, join, neutral, backward):
    count = lax.axis_size(axis)
    place = lax.axis_index(axis)
    ahead = count - 1 - place if backward else place
    gathered = jax.tree.map(
        lambda a, kind: lax.all_gather(a.astype(kind), axis),
        value,
        jax.tree.map(lambda a: jnp.bfloat16 if a.dtype == jnp.float32 else a.dtype, value),
    )
    state = jax.tree.map(lambda a, e: jnp.zeros_like(a) + jnp.asarray(e, a.dtype), value, neutral)

    def one(lap, state):
        source = count - 1 - lap if backward else lap
        return join(
            state,
            jax.tree.map(
                lambda a, own: lax.dynamic_index_in_dim(a, source, 0, False).astype(own.dtype),
                gathered,
                value,
            ),
        )

    return lax.fori_loop(0, ahead, one, state)


def heads_first(values, heads):
    return values.reshape(values.shape[0], heads, -1).transpose(1, 0, 2)


def block_scan(query, key, value, logarithm_fading):
    heads, length, key_size = query.shape
    value_size = value.shape[-1]
    count = length // BLK

    def blocks(tensor):
        return tensor.reshape(heads, count, BLK, tensor.shape[-1])

    qb, kb, vb, gb = (blocks(query), blocks(key), blocks(value), blocks(logarithm_fading))
    cum = jnp.cumsum(gb, axis=2)
    last = cum[:, :, -1:, :]
    q_in = qb * jnp.exp(cum)
    k_in = kb * jnp.exp(-cum)
    k_st = kb * jnp.exp(last - cum)
    lower = jnp.tril(jnp.ones((BLK, BLK), dtype=bool))
    scores = jnp.where(lower, jnp.einsum("hnid,hnjd->hnij", q_in, k_in, precision=highest), 0.0)
    inner = jnp.einsum("hnij,hnjv->hniv", scores, vb, precision=highest)
    growth = jnp.einsum("hnjd,hnjv->hndv", k_st, vb, precision=highest)
    fading_speed = jnp.exp(last[:, :, 0, :])

    def step(state, inputs):
        factor, added = inputs
        return (factor[..., None] * state + added, state)

    final, starts = lax.scan(
        step,
        jnp.zeros((heads, key_size, value_size), jnp.float32),
        (fading_speed.transpose(1, 0, 2), growth.transpose(1, 0, 2, 3)),
    )
    carried = jnp.einsum("hnid,hndv->hniv", q_in, starts.transpose(1, 0, 2, 3), precision=highest)
    return ((inner + carried).reshape(heads, length, value_size), final)


def group_local(query, key, value, fading_speed, key_size):
    heads = query.shape[1] // key_size
    qh = heads_first(query.astype(jnp.float32), heads) * key_size ** (-0.5)
    kh = heads_first(key.astype(jnp.float32), heads)
    vh = heads_first(value.astype(jnp.float32), heads)
    logarithm_fading = jax.nn.log_sigmoid(fading_speed) / normalizer_sharpness
    ahead = heads_first(logarithm_fading[0], heads)
    behind = heads_first(logarithm_fading[1], heads)[:, ::-1]
    flipped_q = qh[:, ::-1]
    forward, state_ahead = block_scan(qh, kh, vh, ahead)
    backward, state_behind = block_scan(flipped_q, kh[:, ::-1], vh[:, ::-1], behind)
    cum_ahead = jnp.cumsum(ahead, axis=1)
    cum_behind = jnp.cumsum(behind, axis=1)
    reader_ahead = qh * jnp.exp(cum_ahead)
    reader_behind = flipped_q * jnp.exp(cum_behind)
    return (
        forward,
        backward,
        reader_ahead,
        reader_behind,
        cum_ahead[:, -1, :],
        cum_behind[:, -1, :],
        state_ahead,
        state_behind,
    )


def chain(earlier, later):
    return (
        earlier[0] + later[0],
        jnp.exp(later[0])[..., None] * earlier[1] + later[1],
        earlier[2] + later[2],
        jnp.exp(later[2])[..., None] * earlier[3] + later[3],
    )


def readout(reader, state):
    return jnp.einsum("htd,hdv->htv", reader, state, precision=highest)


def finish(mixed, gate, head_gain):
    normed = mixed * lax.rsqrt(jnp.mean(mixed * mixed, axis=-1, keepdims=True) + 1e-06) * head_gain
    flat = normed.transpose(1, 0, 2).reshape(mixed.shape[1], -1)
    return (flat * jax.nn.silu(gate.astype(jnp.float32))).astype(jnp.bfloat16)


def layer_norm(values, gain):
    mean = jnp.mean(values, axis=-1, keepdims=True)
    spread = jnp.mean(jnp.square(values - mean), axis=-1, keepdims=True)
    return (values - mean) * lax.rsqrt(spread + 1e-05) * gain


def body(
    query_one,
    key_one,
    value_one,
    gate_one,
    decay_one,
    query_two,
    key_two,
    value_two,
    gate_two,
    decay_two,
    head_gain,
    proj_one,
    proj_two,
    stream,
    gain_mix,
    gain_moe,
    routes,
    affinity,
    expert_gate,
    expert_up,
    expert_down,
):
    rows = query_one.shape[0]
    tp_count = lax.axis_size("tp")
    tp_rank = lax.axis_index("tp")
    sp_count = lax.axis_size("sp")
    own_rows = rows // tp_count
    first = group_local(query_one, key_one, value_one, decay_one, DK_A)
    second = group_local(query_two, key_two, value_two, decay_two, DK_B)
    ahead_in = (first[4], first[6], second[4], second[6])
    behind_in = (first[5], first[7], second[5], second[7])
    empty = tuple((jnp.zeros_like(item) for item in ahead_in))
    from_left = carried_in(ahead_in, "sp", chain, empty, False)
    from_right = carried_in(behind_in, "sp", chain, empty, True)
    mixed_one = (
        first[0]
        + readout(first[2], from_left[1])
        + (first[1] + readout(first[3], from_right[1]))[:, ::-1]
    )
    mixed_two = (
        second[0]
        + readout(second[2], from_left[3])
        + (second[1] + readout(second[3], from_right[3]))[:, ::-1]
    )
    heads_one = finish(mixed_one, gate_one, head_gain)
    heads_two = finish(mixed_two, gate_two, head_gain)
    part = jnp.dot(heads_one, proj_one, preferred_element_type=jnp.float32)
    attn = lax.psum(
        (part + jnp.dot(heads_two, proj_two, preferred_element_type=jnp.float32)).astype(
            jnp.bfloat16
        ),
        "tp",
    )
    settled = layer_norm(stream.astype(jnp.float32) + attn.astype(jnp.float32), gain_mix)
    moe_in = settled.astype(jnp.bfloat16)
    settled_own = lax.dynamic_slice_in_dim(settled, tp_rank * own_rows, own_rows, 0)
    top_count = routes.shape[1]
    local_experts = expert_gate.shape[0]
    expert_total = local_experts * sp_count
    capacity = 3 * rows * top_count // (2 * expert_total)
    width = moe_in.shape[1]
    slice_width = width // tp_count
    flat_expert = routes.reshape(-1)
    weights = affinity / jnp.sum(affinity, axis=-1, keepdims=True)
    flat_weights = weights.reshape(-1)
    onehot = (flat_expert[:, None] == jnp.arange(expert_total, dtype=jnp.int32)[None, :]).astype(
        jnp.int32
    )
    rank = jnp.sum(jnp.cumsum(onehot, axis=0) * onehot, axis=1) - 1
    target = flat_expert * capacity + rank
    token = jnp.arange(rows * top_count, dtype=jnp.int32) // top_count
    outgoing = (
        jnp.zeros((expert_total * capacity, width), jnp.bfloat16).at[target].set(moe_in[token])
    )
    outgoing = outgoing.reshape(sp_count, local_experts, capacity, width)
    received = lax.all_to_all(outgoing, "sp", split_axis=0, concat_axis=0, tiled=True)
    gate = jnp.einsum("secd,edf->secf", received, expert_gate, preferred_element_type=jnp.float32)
    upward = jnp.einsum("secd,edf->secf", received, expert_up, preferred_element_type=jnp.float32)
    act = (jax.nn.silu(gate) * upward).astype(jnp.bfloat16)
    partial_value = jnp.einsum(
        "secf,efd->secd", act, expert_down, preferred_element_type=jnp.float32
    ).astype(jnp.bfloat16)
    summed = lax.psum_scatter(
        partial_value.astype(jnp.float32).astype(jnp.bfloat16),
        "tp",
        scatter_dimension=3,
        tiled=True,
    )
    returned = lax.all_to_all(summed, "sp", split_axis=0, concat_axis=0, tiled=True)
    pieces = returned.reshape(expert_total * capacity, slice_width)[target]
    weighted = pieces.astype(jnp.float32) * flat_weights[:, None]
    term = jnp.sum(weighted.reshape(rows, top_count, slice_width), axis=1)
    mixture = lax.all_to_all(
        term.astype(jnp.bfloat16), "tp", split_axis=0, concat_axis=1, tiled=True
    ).astype(term.dtype)
    return layer_norm(settled_own + mixture, gain_moe).astype(jnp.bfloat16)


def solution(mesh):
    return jax.shard_map(
        body,
        mesh=mesh,
        in_specs=(
            P("sp", "tp"),
            P("sp", "tp"),
            P("sp", "tp"),
            P("sp", "tp"),
            P(None, "sp", "tp"),
            P("sp", "tp"),
            P("sp", "tp"),
            P("sp", "tp"),
            P("sp", "tp"),
            P(None, "sp", "tp"),
            P(),
            P("tp", None),
            P("tp", None),
            P("sp", None),
            P(),
            P(),
            P("sp", None),
            P("sp", None),
            P("sp", None, "tp"),
            P("sp", None, "tp"),
            P("sp", "tp", None),
        ),
        out_specs=P(("sp", "tp"), None),
        check_vma=False,
    )
```

profile of v0, /device:TPU:1, one launch (start us, length us, event | category | flops | bytes accessed | tf_op | source)
XLA Modules:
  0.0 630.3 jit_solution(2608823896840268187)
XLA Ops:
  33.1 7.5 %while.89 = (s32[]{:T(128)}, f32[4,128,128]{2,1,0:T(8,128)S(1)}, f32[4,4,128,128]{3,2,1,0:T(8,128)}, f32[4,4,128]{2,0,1:T(4,128)S(1)}, f32[4,4,128,128]{3,2,0,1:T(8,128)}, /*index=5*/s32[]{:T(128)}, s32[]{:T(128)}) while((s32[]{:T(128)}, f32[4,128,128]{2,1,0:T(8,128)S(1)}, f32[4,4,128,128]{3,2,1,0:T(8,128)}, ...), condition=%wide.region_21.22_spmd.clone, body=%wide.region_20.21_spmd.clone.sunk | while | flops 262147 | bytes 1316972 | solution.py:68
  50.0 7.5 %while.87 = (s32[]{:T(128)}, f32[4,128,128]{2,1,0:T(8,128)S(1)}, f32[4,4,128,128]{3,2,1,0:T(8,128)}, f32[4,4,128]{2,0,1:T(4,128)S(1)}, f32[4,4,128,128]{3,2,0,1:T(8,128)}, /*index=5*/s32[]{:T(128)}, s32[]{:T(128)}) while((s32[]{:T(128)}, f32[4,128,128]{2,1,0:T(8,128)S(1)}, f32[4,4,128,128]{3,2,1,0:T(8,128)}, ...), condition=%wide.region_9.10_spmd.clone, body=%wide.region_8.9_spmd.clone.sunk | while | flops 262147 | bytes 1316972 | solution.py:68
  80.2 5.1 reverse.7
  96.1 4.5 reduce-window.40
  102.0 23.2 %all-gather.4 = bf16[32,1,64]{2,1,0:T(2,128)(2,1)S(1)} all-gather(bf16[4,1,64]{2,1,0:T(2,128)(2,1)S(1)} %copy.298), channel_id=6, replica_groups=mesh['sp'=8,'tp'=4] {'sp'}, dimensions={0}, use_global_device_ids=true | all-gather | bytes 4608 | tf_op jit(solution)/shard_map/all_gather | solution.py:20
  137.1 6.8 %while.88 = (s32[]{:T(128)}, f32[4,64,128]{2,1,0:T(8,128)S(1)}, f32[4,4,64,128]{3,2,1,0:T(8,128)}, f32[4,4,64]{2,0,1:T(4,128)S(1)}, f32[4,4,64,128]{3,2,0,1:T(8,128)}, /*index=5*/s32[]{:T(128)}, s32[]{:T(128)}) while((s32[]{:T(128)}, f32[4,64,128]{2,1,0:T(8,128)S(1)}, f32[4,4,64,128]{3,2,1,0:T(8,128)}, ...), condition=%wide.region_14.15_spmd.clone, body=%wide.region_13.14_spmd.clone.sunk | while | flops 131075 | bytes 658540 | solution.py:68
  144.0 27.2 %all-gather.5 = bf16[32,64,128]{2,1,0:T(8,128)(2,1)} all-gather(bf16[4,64,128]{2,1,0:T(8,128)(2,1)S(1)} %convert_element_type.216), channel_id=7, replica_groups=mesh['sp'=8,'tp'=4] {'sp'}, dimensions={0}, use_global_device_ids=true | all-gather | bytes 589824 | tf_op jit(solution)/shard_map/all_gather | solution.py:20
  174.1 21.8 %all-gather.6 = bf16[32,1,128]{2,1,0:T(2,128)(2,1)S(1)} all-gather(bf16[4,1,128]{2,1,0:T(2,128)(2,1)S(1)} %slice.114), channel_id=8, replica_groups=mesh['sp'=8,'tp'=4] {'sp'}, dimensions={0}, use_global_device_ids=true | all-gather | bytes 9216 | tf_op jit(solution)/shard_map/all_gather | solution.py:20
  212.0 21.5 %all-gather = bf16[32,1,64]{2,1,0:T(2,128)(2,1)S(1)} all-gather(bf16[4,1,64]{2,1,0:T(2,128)(2,1)S(1)} %copy.274), channel_id=2, replica_groups=mesh['sp'=8,'tp'=4] {'sp'}, dimensions={0}, use_global_device_ids=true | all-gather | bytes 4608 | tf_op jit(solution)/shard_map/all_gather | solution.py:20
  240.9 6.9 %while.86 = (s32[]{:T(128)}, f32[4,64,128]{2,1,0:T(8,128)S(1)}, f32[4,4,64,128]{3,2,1,0:T(8,128)}, f32[4,4,64]{2,0,1:T(4,128)S(1)}, f32[4,4,64,128]{3,2,0,1:T(8,128)}, /*index=5*/s32[]{:T(128)}, s32[]{:T(128)}) while((s32[]{:T(128)}, f32[4,64,128]{2,1,0:T(8,128)S(1)}, f32[4,4,64,128]{3,2,1,0:T(8,128)}, f32[4,4,64]{2,0,1:T(4,128)S(1)}, ...), condition=%wide.region_2.3_spmd.clone, body=%wide.region_1.2_spmd.clone.sunk | while | flops 131075 | bytes 658540 | solution.py:68
  247.8 27.4 %all-gather.1 = bf16[32,64,128]{2,1,0:T(8,128)(2,1)} all-gather(bf16[4,64,128]{2,1,0:T(8,128)(2,1)S(1)} %convert_element_type.212), channel_id=3, replica_groups=mesh['sp'=8,'tp'=4] {'sp'}, dimensions={0}, use_global_device_ids=true | all-gather | bytes 589824 | tf_op jit(solution)/shard_map/all_gather | solution.py:20
  281.0 22.1 %all-gather.2 = bf16[32,1,128]{2,1,0:T(2,128)(2,1)S(1)} all-gather(bf16[4,1,128]{2,1,0:T(2,128)(2,1)S(1)} %slice.104), channel_id=4, replica_groups=mesh['sp'=8,'tp'=4] {'sp'}, dimensions={0}, use_global_device_ids=true | all-gather | bytes 9216 | tf_op jit(solution)/shard_map/all_gather | solution.py:20
  324.7 23.8 %while.85 = (s32[]{:T(128)}, f32[4,64,128]{2,1,0:T(8,128)S(1)}, f32[4,128,128]{2,1,0:T(8,128)S(1)}, s32[]{:T(128)}, bf16[8,4,64]{2,1,0:T(4,128)(2,1)}, /*index=5...) while((s32[]{:T(128)}, f32[4,64,128]{2,1,0:T(8,128)S(1)}, ...), condition=%wide.region_23.24_spmd, body=%wide.region_22.23_spmd.sunk | while | flops 295686 | bytes 990907 | solution.py:37
  351.0 5.1 rev.39
  359.7 5.1 rev.37
  374.8 62.9 %all-reduce.2.cloned.1.call-done = bf16[256,2048]{1,0:T(8,128)(2,1)} async-done(((bf16[256,2048]{1,0:T(8,128)(2,1)}), bf16[256,2048]{1,0:T(8,128)(2,1)}) %all-reduce.2.cloned.1.call-update) | async-done | bytes 1048592 | tf_op jit(solution)/shard_map/psum | solution.py:177
  442.1 11.7 %scatter_custom_fusion = bf16[768,2048]{1,0:T(8,128)(2,1)} fusion(s32[512]{0:T(512)S(1)} %bitcast.495, bf16[256,2048]{1,0:T(8,128)(2,1)} %get-tuple-element.576, s32[1024]{0:T(1024)S(1)} %pad_clamp_fusion.1, bf16[]{:T(256)} %constant.209.clone.1), kind=kCustom, calls=%fused_computation.35 | custom fusion | bytes 3146240 | tf_op jit(solution)/shard_map/scatter | solution.py:202
  453.8 75.2 %all_to_all.20 = bf16[8,1,96,2048]{3,2,1,0:T(8,128)(2,1)S(1)} all-to-all(bf16[8,1,96,2048]{3,2,1,0:T(8,128)(2,1)} %bitcast.417), channel_id=1, replica_groups=mesh['sp'=8,'tp'=4] {'sp'}, dimensions={0} | all-to-all | bytes 6291456 | tf_op jit(solution)/shard_map/all_to_all | solution.py:205
  533.7 8.1 %fusion.4 = bf16[8,1,96,2048]{3,2,0,1:T(8,128)(2,1)} fusion(bf16[1,512,2048]{2,1,0:T(8,128)(2,1)S(1)} %copy-done, bf16[1,2048,512]{2,1,0:T(8,128)(2,1)} %param.52, bf16[8,1,96,2048]{3,2,1,0:T(8,128)(2,1)} %copy-done.23, f32[8,96,512]{2,1,0:T(8,128)} %fusion.2), kind=kOutput, calls=%fused_computation.29 | convolution fusion | flops 3225157632 | bytes 12058624 | tf_op jit(solution)/shard_map/secf,efd->secd/dot_general | solution.py:209
  541.8 37.8 %reduce-scatter.2.cloned.1.call-done = bf16[8,1,96,512]{3,2,0,1:T(8,128)(2,1)} async-done(((bf16[8,1,96,2048]{3,2,0,1:T(8,128)(2,1)}), bf16[8,1,96,512]{3,2,0,1:T(8,128)(2,1)}) %reduce-scatter.2.cloned.1.call-update) | async-done | bytes 786448 | tf_op jit(solution)/shard_map/reduce_scatter | solution.py:212
  579.6 5.2 all-to-all-start.1
  585.0 18.9 %all-to-all-done.1 = bf16[8,1,96,512]{3,2,1,0:T(8,128)(2,1)S(1)} async-done(((bf16[8,1,96,512]{3,2,1,0:T(8,128)(2,1)}), bf16[8,1,96,512]{3,2,1,0:T(8,128)(2,1)S(1)}, u32[]{:S(2)}, u32[]{:S(2)}) %all-to-all-start.1) | async-done | bytes 786464 | tf_op jit(solution)/shard_map/all_to_all | solution.py:218
  610.3 5.5 all-to-all-start.2
  615.8 5.0 all-to-all-done.2
  (378 shorter events, 221.7 us)
Async XLA Ops:
  6.5 527.2 %copy-start = (bf16[1,512,2048]{2,1,0:T(8,128)(2,1)S(1)}, bf16[1,512,2048]{2,1,0:T(8,128)(2,1)}, u32[]{:S(2)}) copy-start(bf16[1,512,2048]{2,1,0:T(8,128)(2,1)} %param.53) | copy-start | bytes 6291460
  6.5 318.1 %all-gather.13.cloned.1.call-start = ((), (), s32[]{:S(2)}) async-start(), calls=%async_computation.7 | async-start | bytes 1179648 | tf_op jit(solution)/shard_map/all_gather | solution.py:20
  8.7 19.4 %copy-start.6 = (f32[4,256,128]{2,1,0:T(8,128)}, f32[4,256,128]{2,1,0:T(8,128)S(1)}, u32[]{:S(2)}) copy-start(f32[4,256,128]{2,1,0:T(8,128)S(1)} %rev.35) | copy-start | bytes 1572868
  18.1 8.4 %copy-start.11 = (f32[4,256,128]{1,2,0:T(8,128)}, f32[4,256,128]{1,2,0:T(8,128)S(1)}, u32[]{:S(2)}) copy-start(f32[4,256,128]{1,2,0:T(8,128)S(1)} %rev.34) | copy-start | bytes 1572868
  33.1 8.2 %copy-start.17 = (f32[1,256,512]{1,2,0:T(8,128)S(1)}, f32[1,256,512]{1,2,0:T(8,128)}, u32[]{:S(2)}) copy-start(f32[1,256,512]{1,2,0:T(8,128)} %get-tuple-element.578) | copy-start | bytes 1572868
  41.3 314.8 %all-gather.11.cloned.1.call-start = ((), (), s32[]{:S(2)}) async-start(), calls=%async_computation.6 | async-start | bytes 1179648 | tf_op jit(solution)/shard_map/all_gather | solution.py:20
  50.0 8.8 %copy-start.47 = (s32[256,2]{0,1:T(2,128)S(1)}, s32[256,2]{0,1:T(2,128)}, u32[]{:S(2)}) copy-start(s32[256,2]{0,1:T(2,128)} %param.49) | copy-start | bytes 6148
  58.2 379.5 %all-reduce.2.cloned.1.call-start = ((), (), s32[]{:S(2)}) async-start(), calls=%async_computation.4 | async-start | bytes 2097152 | tf_op jit(solution)/shard_map/psum | solution.py:177
  71.0 18.2 %copy-start.30 = (bf16[256,256]{0,1:T(8,128)(2,1)}, bf16[256,256]{0,1:T(8,128)(2,1)S(1)}, u32[]{:S(2)}) copy-start(bf16[256,256]{0,1:T(8,128)(2,1)S(1)} %copy.258) | copy-start | bytes 393220
  71.0 18.2 %copy-start.7 = (f32[4,256,128]{2,1,0:T(8,128)S(1)}, f32[4,256,128]{2,1,0:T(8,128)}, u32[]{:S(2)}) copy-start(f32[4,256,128]{2,1,0:T(8,128)} %copy-done.6) | copy-start | bytes 1572868
  80.2 11.3 %copy-start.43 = (s32[8,5]{0,1:T(8,128)}, s32[8,5]{0,1:T(8,128)S(1)}, u32[]{:S(2)}) copy-start(s32[8,5]{0,1:T(8,128)S(1)} %reduce-window.49) | copy-start | bytes 484
  94.0 31.8 %copy-start.35 = (f32[4,256,64]{2,1,0:T(8,128)S(1)}, f32[4,256,64]{2,1,0:T(8,128)}, u32[]{:S(2)}) copy-start(f32[4,256,64]{2,1,0:T(8,128)} %copy.339) | copy-start | bytes 786436
  137.1 34.0 %copy-start.12 = (f32[4,256,128]{1,2,0:T(8,128)S(1)}, f32[4,256,128]{1,2,0:T(8,128)}, u32[]{:S(2)}) copy-start(f32[4,256,128]{1,2,0:T(8,128)} %copy-done.11) | copy-start | bytes 1572868
  174.1 27.4 %copy-start.2 = (f32[4,4,64,128]{3,2,1,0:T(8,128)S(1)}, f32[4,4,64,128]{3,2,1,0:T(8,128)}, u32[]{:S(2)}) copy-start(f32[4,4,64,128]{3,2,1,0:T(8,128)} %copy-done.1) | copy-start | bytes 1572868
  324.6 23.9 %copy-start.36 = (f32[4,256,128]{1,2,0:T(8,128)S(1)}, f32[4,256,128]{1,2,0:T(8,128)}, u32[]{:S(2)}) copy-start(f32[4,256,128]{1,2,0:T(8,128)} %copy.322) | copy-start | bytes 1572868
  324.7 23.9 %copy-start.18 = (f32[4,256,128]{1,2,0:T(8,128)S(1)}, f32[4,256,128]{1,2,0:T(8,128)}, u32[]{:S(2)}) copy-start(f32[4,256,128]{1,2,0:T(8,128)} %reverse.7) | copy-start | bytes 1572868
  356.2 8.6 %copy-start.20 = (bf16[256,512]{0,1:T(8,128)(2,1)S(1)}, bf16[256,512]{0,1:T(8,128)(2,1)}, u32[]{:S(2)}) copy-start(bf16[256,512]{0,1:T(8,128)(2,1)} %copy-done.19) | copy-start | bytes 786436
  372.6 65.1 %copy-start.3 = (bf16[256,2048]{1,0:T(8,128)(2,1)S(1)}, bf16[256,2048]{1,0:T(8,128)(2,1)}, u32[]{:S(2)}) copy-start(bf16[256,2048]{1,0:T(8,128)(2,1)} %param.46) | copy-start | bytes 3145732
  374.4 205.2 %reduce-scatter.2.cloned.1.call-start = ((), (), s32[]{:S(2)}) async-start(), calls=%async_computation.5 | async-start | bytes 3932160 | tf_op jit(solution)/shard_map/reduce_scatter | solution.py:212
  374.8 65.2 %copy-start.44 = (f32[2048]{0:T(1024)S(1)}, f32[2048]{0:T(1024)}, u32[]{:S(2)}) copy-start(f32[2048]{0:T(1024)} %param.47) | copy-start | bytes 24580
  453.8 76.9 %copy-start.52 = (bf16[1,2048,512]{2,1,0:T(8,128)(2,1)S(1)}, bf16[1,2048,512]{2,1,0:T(8,128)(2,1)}, u32[]{:S(2)}) copy-start(bf16[1,2048,512]{2,1,0:T(8,128)(2,1)} %param.51) | copy-start | bytes 6291460
  541.8 43.1 %copy-start.50 = (f32[256,2]{0,1:T(2,128)S(1)}, f32[256,2]{0,1:T(2,128)}, u32[]{:S(2)}) copy-start(f32[256,2]{0,1:T(2,128)} %param.50) | copy-start | bytes 6148
  579.6 24.3 %all-to-all-start.1 = ((bf16[8,1,96,512]{3,2,1,0:T(8,128)(2,1)}), bf16[8,1,96,512]{3,2,1,0:T(8,128)(2,1)S(1)}, u32[]{:S(2)}, u32[]{:S(2)}) async-start(bf16[8,1,96,512]{3,2,1,0:T(8,128)(2,1)} %bitcast.471), calls=%async_computation.2 | async-start | bytes 1572864 | tf_op jit(solution)/shard_map/all_to_all | solution.py:218
  610.3 10.5 %all-to-all-start.2 = ((bf16[4,64,512]{2,1,0:T(8,128)(2,1)}), bf16[4,64,512]{2,1,0:T(8,128)(2,1)S(1)}, u32[]{:S(2)}, u32[]{:S(2)}) async-start(bf16[4,64,512]{2,1,0:T(8,128)(2,1)} %bitcast.122), calls=%async_computation.3 | async-start | bytes 524288 | tf_op jit(solution)/shard_map/all_to_all | solution.py:222
  (37 other events, 110.3 us)
Sparse Core Ops, SparseCore 0:
  41.4 40.6 all-gather.12
  84.2 39.2 all-gather.10
  374.5 63.1 all-reduce.1
  541.9 37.6 reduce-scatter.1
where the time goes:
time: 641 us; the launch traced here: 630 us
  blocking collectives  218 us (34%)
  waiting for transfers between devices  125 us (20%)
  local copies, waits for them, and re-layouts  109 us (17%)
  other arithmetic  98.6 us (15%)
  matrix products  52.9 us (8%)
  between operations  14.7 us (2%)
  starting transfers between devices  11.6 us (2%)
    all_gather x6, blocking collectives, carried_in(): lax.all_gather(a.astype(kind), axis)  143 us
    all_to_all x1, blocking collectives, body(): lax.all_to_all(outgoing, 'sp', split_axis=0, concat_axis=0, tiled=True)  75.2 us
    psum x1, waiting for transfers between devices, body(): lax.psum((part + jnp.dot(heads_two, proj_two, preferred_element_type=jnp....  62.9 us
    reduce_scatter x1, waiting for transfers between devices, body(): lax.psum_scatter(partial_value.astype(jnp.float32).astype(jnp.bfloat16),...  37.8 us
    all_to_all x1, waiting for transfers between devices, body(): lax.all_to_all(summed, 'sp', split_axis=0, concat_axis=0, tiled=True)  18.9 us
    add x16, other arithmetic, step(): return (factor[..., None] * state + added, state)  17.1 us
    another operation x30, local copies, waits for them, and re-layouts  16 us
    another operation x10, other arithmetic  13 us
  transfers between devices with their start and end apart: 6, of which 4 were waited for; matrix products, arithmetic and copies ran while one was open for 27% of the time, Pallas kernels for 0%

commit v1 on v0

v1 whole, which is shorter than its diff:
```python
import functools

import jax
import jax.numpy as jnp
from jax import lax
from jax.experimental import pallas as pl
from jax.experimental.pallas import tpu as pltpu
from jax.sharding import PartitionSpec as P

DK_A = 64
DK_B = 128
BLK = 64
SHARPNESS = 16.0
F32 = jnp.float32
BF16 = jnp.bfloat16
MESH = pl.DeviceIdType.MESH
VMEM = pl.BlockSpec(memory_space=pltpu.VMEM)
DMA = pltpu.SemaphoreType.DMA


def params(collective_id=None):
    if collective_id is None:
        return pltpu.CompilerParams(vmem_limit_bytes=48 * 2**20)
    return pltpu.CompilerParams(
        vmem_limit_bytes=48 * 2**20, collective_id=collective_id, has_side_effects=True
    )


def mm(a, b):
    return jnp.dot(a, b, preferred_element_type=F32)


def mm_nt(a, b):
    return lax.dot_general(a, b, (((1,), (1,)), ((), ())), preferred_element_type=F32)


def mm_tn(a, b):
    return lax.dot_general(a, b, (((0,), (0,)), ((), ())), preferred_element_type=F32)


def log_sigmoid(x):
    return jnp.minimum(x, 0.0) - jnp.log1p(jnp.exp(-jnp.abs(x)))


def silu(x):
    return x / (1.0 + jnp.exp(-x))


def layer_norm(values, gain):
    mean = jnp.mean(values, axis=-1, keepdims=True)
    spread = jnp.mean(jnp.square(values - mean), axis=-1, keepdims=True)
    return (values - mean) * lax.rsqrt(spread + 1e-05) * gain


def greet(peers):
    barrier = pltpu.get_barrier_semaphore()
    for peer in peers:
        pl.semaphore_signal(barrier, inc=1, device_id=peer, device_id_type=MESH)
    pl.semaphore_wait(barrier, len(peers))


def remote(src, dst, send, recv, peer):
    return pltpu.make_async_remote_copy(
        src_ref=src, dst_ref=dst, send_sem=send, recv_sem=recv, device_id=peer, device_id_type=MESH
    )


def state_kernel(ka, va, da, kb, vb, db, stack, cum):
    rows = ka.shape[0]
    count = rows // BLK
    ii = lax.broadcasted_iota(jnp.int32, (rows, rows), 0)
    jj = lax.broadcasted_iota(jnp.int32, (rows, rows), 1)
    same = (ii // BLK) == (jj // BLK)
    lower = jnp.where(same & (ii >= jj), 1.0, 0.0).astype(BF16)
    upper = jnp.where(same & (ii <= jj), 1.0, 0.0).astype(BF16)
    base = 0
    for k, v, d, dk in ((ka, va, da, DK_A), (kb, vb, db, DK_B)):
        wide = k.shape[1]
        heads = wide // dk
        dv = v.shape[1] // heads
        keys = k[...].astype(F32)
        for way in range(2):
            fade = log_sigmoid(d[way]) / SHARPNESS
            high = fade.astype(BF16)
            low = (fade - high.astype(F32)).astype(BF16)
            tri = lower if way == 0 else upper
            total = mm(tri, high) + mm(tri, low)
            cum[way, :, base : base + wide] = total
            tail = jnp.zeros((1, wide), F32)
            weighted = [None] * count
            for b in reversed(range(count)) if way == 0 else range(count):
                part = total[b * BLK : (b + 1) * BLK]
                last = part[BLK - 1 : BLK] if way == 0 else part[0:1]
                weighted[b] = (keys[b * BLK : (b + 1) * BLK] * jnp.exp(last - part + tail)).astype(BF16)
                tail = tail + last
            weighted = jnp.concatenate(weighted, axis=0)
            states = [
                mm_tn(v[:, h * dv : (h + 1) * dv], weighted[:, h * dk : (h + 1) * dk]).astype(BF16)
                for h in range(heads)
            ]
            stack[way, 0:dv, base : base + wide] = (
                states[0] if heads == 1 else jnp.concatenate(states, axis=1)
            )
            thigh = tail.astype(BF16).astype(F32)
            row = lax.broadcasted_iota(jnp.int32, (16, wide), 0)
            stack[way, dv : dv + 16, base : base + wide] = jnp.where(
                row == 0, thigh, jnp.where(row == 1, tail - thigh, 0.0)
            ).astype(BF16)
        base += wide


def states_exchange_kernel(n, x, out, send, recv):
    me = lax.axis_index("sp")
    greet([{"sp": lax.rem(me + k, n)} for k in range(1, n)])
    copies = []
    for k in range(1, n):
        peer = lax.rem(me + k, n)
        way = jnp.where(peer < me, 1, 0)
        copy = remote(x.at[way], out.at[me], send.at[k], recv.at[k], {"sp": peer})
        copy.start()
        copies.append(copy)
    for k in range(1, n):
        peer = lax.rem(me + k, n)
        copies[k - 1].wait_send()
        remote(x.at[0], out.at[lax.rem(me + n - k, n)], send.at[k], recv.at[k], {"sp": peer}).wait_recv()


def mix_kernel(
    n, states, cum, qa, ka, va, ga, qb, kb, vb, gb, gain, pa, pb, out, heads_ref, ahead, behind
):
    me = lax.axis_index("sp")
    rows = qa.shape[0]
    count = rows // BLK
    dv = ahead.shape[0]
    ahead[...] = jnp.zeros_like(ahead)
    behind[...] = jnp.zeros_like(behind)

    def join(total, source):
        fade = states[source, dv : dv + 1, :].astype(F32) + states[source, dv + 1 : dv + 2, :].astype(F32)
        total[...] = jnp.exp(fade) * total[...] + states[source, 0:dv, :].astype(F32)

    def one(s, carry):
        @pl.when(s < me)
        def _():
            join(ahead, s)

        back = n - 1 - s

        @pl.when(back > me)
        def _():
            join(behind, back)

        return carry

    lax.fori_loop(0, n, one, 0)
    ii = lax.broadcasted_iota(jnp.int32, (BLK, BLK), 0)
    jj = lax.broadcasted_iota(jnp.int32, (BLK, BLK), 1)
    base = 0
    column = 0
    for q, k, v, g, dk in ((qa, ka, va, ga, DK_A), (qb, kb, vb, gb, DK_B)):
        heads = q.shape[1] // dk
        for h in range(heads):
            lanes = slice(base + h * dk, base + (h + 1) * dk)
            own = slice(h * dk, (h + 1) * dk)
            vown = slice(h * dv, (h + 1) * dv)
            forward = ahead[:, lanes]
            backward = behind[:, lanes]
            mixed = [None] * count
            readers = [None] * count
            growth = [None] * count
            for b in range(count):
                at = slice(b * BLK, (b + 1) * BLK)
                query = q[at, own].astype(F32) * dk ** (-0.5)
                key = k[at, own].astype(F32)
                value = v[at, vown]
                cf = cum[0, at, lanes]
                cb = cum[1, at, lanes]
                qf = (query * jnp.exp(cf)).astype(BF16)
                kf = (key * jnp.exp(-cf)).astype(BF16)
                qr = (query * jnp.exp(cb)).astype(BF16)
                kr = (key * jnp.exp(-cb)).astype(BF16)
                scores = jnp.where(ii >= jj, mm_nt(qf, kf), 0.0) + jnp.where(ii <= jj, mm_nt(qr, kr), 0.0)
                inner = mm(scores.astype(BF16), value)
                lastf = cf[BLK - 1 : BLK]
                inner = inner + mm_nt(qf, forward.astype(BF16))
                if b < count - 1:
                    kfs = (key * jnp.exp(lastf - cf)).astype(BF16)
                    forward = jnp.exp(lastf) * forward + mm_tn(value, kfs)
                mixed[b] = inner
                readers[b] = qr
                lastb = cb[0:1]
                if b > 0:
                    kbs = (key * jnp.exp(lastb - cb)).astype(BF16)
                    growth[b] = (jnp.exp(lastb), mm_tn(value, kbs))
            for b in reversed(range(count)):
                at = slice(b * BLK, (b + 1) * BLK)
                whole = mixed[b] + mm_nt(readers[b], backward.astype(BF16))
                if b > 0:
                    backward = growth[b][0] * backward + growth[b][1]
                scale = lax.rsqrt(jnp.mean(whole * whole, axis=-1, keepdims=True) + 1e-06)
                heads_ref[at, column + h * dv : column + (h + 1) * dv] = (
                    whole * scale * gain[...] * silu(g[at, vown].astype(F32))
                ).astype(BF16)
        base += heads * dk
        column += heads * dv
    split = pa.shape[0]
    width = out.shape[1]
    tile = min(512, width)
    for j in range(width // tile):
        cols = slice(j * tile, (j + 1) * tile)
        out[:, cols] = (
            mm(heads_ref[:, :split], pa[:, cols]) + mm(heads_ref[:, split:], pb[:, cols])
        ).astype(BF16)


def settle_kernel(n, part, stream, gain, settled, columns, inbox, outbox, send, recv, send2, recv2):
    me = lax.axis_index("tp")
    own = part.shape[0] // n
    wide = part.shape[1] // n
    greet([{"tp": lax.rem(me + k, n)} for k in range(1, n)])

    def rows_of(i):
        return pl.ds(pl.multiple_of(i * own, own), own)

    def cols_of(i):
        return pl.ds(pl.multiple_of(i * wide, wide), wide)

    copies = []
    for k in range(1, n):
        peer = lax.rem(me + k, n)
        copy = remote(part.at[rows_of(peer), :], inbox.at[k], send.at[k], recv.at[k], {"tp": peer})
        copy.start()
        copies.append(copy)
    total = part[rows_of(me), :].astype(F32)
    for k in range(1, n):
        copies[k - 1].wait_recv()
        total = total + inbox[k].astype(F32)
    total = total.astype(BF16).astype(F32)
    value = layer_norm(stream[rows_of(me), :].astype(F32) + total, gain[...])
    settled[...] = value
    outbox[...] = value.astype(BF16)
    second = []
    for k in range(1, n):
        peer = lax.rem(me + k, n)
        copy = remote(
            outbox.at[:, cols_of(peer)], columns.at[rows_of(me), :], send2.at[k], recv2.at[k], {"tp": peer}
        )
        copy.start()
        second.append(copy)
    columns[rows_of(me), :] = outbox[:, cols_of(me)]
    for k in range(1, n):
        source = lax.rem(me + n - k, n)
        copies[k - 1].wait_send()
        second[k - 1].wait_send()
        remote(
            outbox.at[:, cols_of(source)], columns.at[rows_of(source), :], send2.at[k], recv2.at[k], {"tp": source}
        ).wait_recv()


def slots_of(routes, capacity, experts):
    rows, top = routes.shape
    lane = lax.broadcasted_iota(jnp.int32, (rows, max(128, experts)), 1)
    hots = [routes[:, i : i + 1] == lane for i in range(top)]
    named = sum(jnp.where(h, 1.0, 0.0) for h in hots)
    ii = lax.broadcasted_iota(jnp.int32, (rows, rows), 0)
    jj = lax.broadcasted_iota(jnp.int32, (rows, rows), 1)
    before = mm(jnp.where(ii > jj, 1.0, 0.0).astype(BF16), named.astype(BF16))
    slots = []
    for i in range(top):
        rank = jnp.sum(jnp.where(hots[i], before, 0.0), axis=1, keepdims=True).astype(jnp.int32)
        slots.append(routes[:, i : i + 1] * capacity + rank)
    return slots


def pick_kernel(capacity, experts, routes, columns, out):
    slots = slots_of(routes[...], capacity, experts)
    rows = columns.shape[0]
    lane = lax.broadcasted_iota(jnp.int32, (rows, experts * capacity), 1)
    hot = sum(jnp.where(lane == s, 1.0, 0.0) for s in slots).astype(BF16)
    out[...] = mm_tn(hot, columns[...]).astype(BF16)


def dispatch_kernel(n, m, x, out, ss, sr, ys, yr, cs, cr, fs, fr, local):
    me = lax.axis_index("sp")
    my = lax.axis_index("tp")
    wide = x.shape[2]
    core = lax.rem(my, 2)
    line = my // 2
    lines = m // 2
    partner = my + 1 - 2 * core

    def cols_of(i):
        return pl.ds(pl.multiple_of(i * wide, wide), wide)

    def line_peer(j):
        return lax.rem(line + j, lines) * 2 + core

    def line_source(j):
        return lax.rem(line + lines - j, lines) * 2 + core

    greet(
        [{"sp": lax.rem(me + k, n)} for k in range(1, n)]
        + [{"tp": partner}]
        + [{"tp": line_peer(j)} for j in range(1, lines)]
    )

    def cross(k):
        peer = lax.rem(me + k, n)
        return remote(x.at[peer], out.at[me, :, cols_of(my)], ss.at[k], sr.at[k], {"sp": peer})

    for k in range(1, n):
        cross(k).start()
    own = pltpu.make_async_copy(x.at[me], out.at[me, :, cols_of(my)], local)
    own.start()

    def block(s, i):
        return out.at[s, :, cols_of(i)]

    def to_line(k, s, j, i):
        return remote(block(s, i), block(s, i), ys.at[k, j], yr.at[k, j], {"tp": line_peer(j)})

    def to_core(k, s, i):
        return remote(block(s, i), block(s, i), cs.at[k], cr.at[k], {"tp": partner})

    def forward(k, s, j, i):
        return remote(block(s, i), block(s, i), fs.at[k, j], fr.at[k, j], {"tp": partner})

    def source(k):
        return lax.rem(me + n - k, n)

    def hand_on(k, s):
        for j in range(1, lines):
            to_line(k, s, j, my).start()
        to_core(k, s, my).start()

    def pass_on(k, s):
        for j in range(1, lines):
            i = line_source(j)
            to_line(k, s, j, i).wait_recv()
            forward(k, s, j, i).start()

    own.wait()
    hand_on(0, me)
    for k in range(1, n):
        s = source(k)
        remote(x.at[0], block(s, my), ss.at[k], sr.at[k], {"sp": s}).wait_recv()
        hand_on(k, s)
        pass_on(k - 1, source(k - 1))
    pass_on(n - 1, source(n - 1))
    for k in range(n):
        s = source(k)
        if k > 0:
            cross(k).wait_send()
        to_core(k, s, my).wait_send()
        to_core(k, s, partner).wait_recv()
        for j in range(1, lines):
            i = line_source(j)
            to_line(k, s, j, my).wait_send()
            forward(k, s, j, i).wait_send()
            forward(k, s, j, i + 1 - 2 * core).wait_recv()


def return_kernel(n, m, x, out, inbox, mid, midbox, last, cs, cr, ys, yr, ss, sr):
    me = lax.axis_index("sp")
    my = lax.axis_index("tp")
    wide = out.shape[2]
    core = lax.rem(my, 2)
    line = my // 2
    lines = m // 2
    partner = my + 1 - 2 * core

    def cols_of(i):
        return pl.ds(pl.multiple_of(i * wide, wide), wide)

    def line_at(j):
        return lax.rem(line + j, lines)

    greet(
        [{"sp": lax.rem(me + k, n)} for k in range(1, n)]
        + [{"tp": partner}]
        + [{"tp": line_at(j) * 2 + core} for j in range(1, lines)]
    )

    def place(k):
        return lax.rem(me + k + 1, n)

    def to_core(k, j):
        i = line_at(j) * 2 + 1 - core
        return remote(x.at[place(k), :, cols_of(i)], inbox.at[k, j], cs.at[k, j], cr.at[k, j], {"tp": partner})

    def to_line(k, j):
        return remote(
            mid.at[k, j], midbox.at[k, j], ys.at[k, j], yr.at[k, j], {"tp": line_at(j) * 2 + core}
        )

    def cross(k):
        peer = place(k)
        return remote(last.at[k], out.at[me], ss.at[k], sr.at[k], {"sp": peer})

    for k in range(n):
        for j in reversed(range(lines)):
            to_core(k, j).start()

    def first(k):
        for j in reversed(range(lines)):
            to_core(k, j).wait_recv()
            i = line_at(j) * 2 + core
            mine = x[place(k), :, cols_of(i)].astype(F32) + inbox[k, j].astype(F32)
            mid[k, j] = mine.astype(BF16)
            if j > 0:
                to_line(k, j).start()

    def second(k):
        total = mid[k, 0].astype(F32)
        for j in range(1, lines):
            to_line(k, j).wait_recv()
            total = total + midbox[k, j].astype(F32)
        if k < n - 1:
            last[k] = total.astype(BF16)
            cross(k).start()
        else:
            out[me] = total.astype(BF16)

    first(0)
    for k in range(1, n):
        first(k)
        second(k - 1)
    second(n - 1)
    for k in range(n):
        for j in range(lines):
            to_core(k, j).wait_send()
            if j > 0:
                to_line(k, j).wait_send()
        if k < n - 1:
            cross(k).wait_send()
            s = lax.rem(me + 2 * n - k - 1, n)
            remote(last.at[k], out.at[s], ss.at[k], sr.at[k], {"sp": s}).wait_recv()


def finish_kernel(n, capacity, experts, routes, affinity, pieces, settled, gain, out, term, mixture, send, recv):
    me = lax.axis_index("tp")
    rows = routes.shape[0]
    own = rows // n
    wide = pieces.shape[1]
    greet([{"tp": lax.rem(me + k, n)} for k in range(1, n)])

    def rows_of(i):
        return pl.ds(pl.multiple_of(i * own, own), own)

    def cols_of(i):
        return pl.ds(pl.multiple_of(i * wide, wide), wide)

    slots = slots_of(routes[...], capacity, experts)
    weights = affinity[...] / jnp.sum(affinity[...], axis=-1, keepdims=True)
    lane = lax.broadcasted_iota(jnp.int32, (rows, experts * capacity), 1)
    total = jnp.zeros((rows, wide), F32)
    for i, slot in enumerate(slots):
        hot = jnp.where(lane == slot, 1.0, 0.0).astype(BF16)
        total = total + weights[:, i : i + 1] * mm(hot, pieces[...])
    term[...] = total.astype(BF16)
    copies = []
    for k in range(1, n):
        peer = lax.rem(me + k, n)
        copy = remote(term.at[rows_of(peer), :], mixture.at[:, cols_of(me)], send.at[k], recv.at[k], {"tp": peer})
        copy.start()
        copies.append(copy)
    mixture[:, cols_of(me)] = term[rows_of(me), :]
    for k in range(1, n):
        source = lax.rem(me + n - k, n)
        copies[k - 1].wait_send()
        remote(
            term.at[rows_of(source), :], mixture.at[:, cols_of(source)], send.at[k], recv.at[k], {"tp": source}
        ).wait_recv()
    out[...] = layer_norm(settled[...] + mixture[...].astype(F32), gain[...]).astype(BF16)


def call(kernel, outs, scratch, count, collective_id=None):
    single = not isinstance(outs, list)
    return pl.pallas_call(
        kernel,
        out_shape=outs,
        in_specs=[VMEM] * count,
        out_specs=VMEM if single else [VMEM] * len(outs),
        scratch_shapes=scratch,
        compiler_params=params(collective_id),
    )


def body(
    query_one,
    key_one,
    value_one,
    gate_one,
    decay_one,
    query_two,
    key_two,
    value_two,
    gate_two,
    decay_two,
    head_gain,
    proj_one,
    proj_two,
    stream,
    gain_mix,
    gain_moe,
    routes,
    affinity,
    expert_gate,
    expert_up,
    expert_down,
):
    shape = jax.ShapeDtypeStruct
    rows = query_one.shape[0]
    n = lax.axis_size("sp")
    m = lax.axis_size("tp")
    width = stream.shape[1]
    own = rows // m
    wide = width // m
    dv = head_gain.shape[0]
    lanes = query_one.shape[1] + query_two.shape[1]
    values = value_one.shape[1] + value_two.shape[1]
    local_experts = expert_gate.shape[0]
    experts = local_experts * n
    top = routes.shape[1]
    capacity = 3 * rows * top // (2 * experts)
    room = local_experts * capacity

    stack, cum = call(
        state_kernel, [shape((2, dv + 16, lanes), BF16), shape((2, rows, lanes), F32)], [], 6
    )(key_one, value_one, decay_one, key_two, value_two, decay_two)
    states = call(
        functools.partial(states_exchange_kernel, n),
        shape((n, dv + 16, lanes), BF16),
        [DMA((n,)), DMA((n,))],
        1,
        1,
    )(stack)
    part = call(
        functools.partial(mix_kernel, n),
        shape((rows, width), BF16),
        [pltpu.VMEM((rows, values), BF16), pltpu.VMEM((dv, lanes), F32), pltpu.VMEM((dv, lanes), F32)],
        13,
    )(
        states, cum, query_one, key_one, value_one, gate_one, query_two, key_two, value_two, gate_two,
        head_gain.reshape(1, -1), proj_one, proj_two,
    )
    settled, columns = call(
        functools.partial(settle_kernel, m),
        [shape((own, width), F32), shape((rows, wide), BF16)],
        [pltpu.VMEM((m, own, width), BF16), pltpu.VMEM((own, width), BF16)] + [DMA((m,))] * 4,
        3,
        2,
    )(part, stream, gain_mix.reshape(1, -1))
    outgoing = call(
        functools.partial(pick_kernel, capacity, experts), shape((experts * capacity, wide), BF16), [], 2
    )(routes, columns)
    lines = m // 2
    received = call(
        functools.partial(dispatch_kernel, n, m),
        shape((n, room, width), BF16),
        [DMA((n,)), DMA((n,)), DMA((n, lines)), DMA((n, lines)), DMA((n,)), DMA((n,)),
         DMA((n, lines)), DMA((n, lines)), DMA],
        1,
        3,
    )(outgoing.reshape(n, room, wide))
    x = received.reshape(n, local_experts, capacity, width)
    results = []
    for e in range(local_experts):
        xe = x[:, e].reshape(n * capacity, width)
        gate = mm(xe, expert_gate[e])
        upward = mm(xe, expert_up[e])
        act = (jax.nn.silu(gate) * upward).astype(BF16)
        results.append(mm(act, expert_down[e]).astype(BF16).reshape(n, capacity, width))
    partial_value = results[0] if local_experts == 1 else jnp.concatenate(results, axis=1)
    pieces = call(
        functools.partial(return_kernel, n, m),
        shape((n, room, wide), BF16),
        [pltpu.VMEM((n, lines, room, wide), BF16)] * 3
        + [pltpu.VMEM((n, room, wide), BF16)]
        + [DMA((n, lines))] * 4
        + [DMA((n,))] * 2,
        1,
        4,
    )(partial_value)
    return call(
        functools.partial(finish_kernel, m, capacity, experts),
        shape((own, width), BF16),
        [pltpu.VMEM((rows, wide), BF16), pltpu.VMEM((own, width), BF16), DMA((m,)), DMA((m,))],
        5,
        5,
    )(routes, affinity, pieces.reshape(experts * capacity, wide), settled, gain_moe.reshape(1, -1))


def solution(mesh):
    return jax.shard_map(
        body,
        mesh=mesh,
        in_specs=(
            P("sp", "tp"),
            P("sp", "tp"),
            P("sp", "tp"),
            P("sp", "tp"),
            P(None, "sp", "tp"),
            P("sp", "tp"),
            P("sp", "tp"),
            P("sp", "tp"),
            P("sp", "tp"),
            P(None, "sp", "tp"),
            P(),
            P("tp", None),
            P("tp", None),
            P("sp", None),
            P(),
            P(),
            P("sp", None),
            P("sp", None),
            P("sp", None, "tp"),
            P("sp", None, "tp"),
            P("sp", "tp", None),
        ),
        out_specs=P(("sp", "tp"), None),
        check_vma=False,
    )
```

time: 641 us -> 171 us (0.27); the launches traced: 630 us -> 170 us
  blocking collectives: 218 us -> 0 us
  Pallas kernels: 0 us -> 145 us
  waiting for transfers between devices: 125 us -> 0 us
  other arithmetic: 98.6 us -> 0 us
  local copies, waits for them, and re-layouts: 109 us -> 13.9 us
  matrix products: 52.9 us -> 11.1 us
  between operations: 14.7 us -> 0.27 us
  starting transfers between devices: 11.6 us -> 0 us
    pallas_call x0 -> x8, Pallas kernels: none -> 145 us  [the longest x1 40.3 us: body(): call(functools.partial(dispatch_kernel, n, m), shape((n, room, width), BF...]
    all_gather x6 -> x0, blocking collectives: 143 us -> none  [carried_in(): lax.all_gather(a.astype(kind), axis)]
    all_to_all x1 -> x0, blocking collectives: 75.2 us -> none  [body(): lax.all_to_all(outgoing, 'sp', split_axis=0, concat_axis=0, tiled=True)]
    psum x1 -> x0, waiting for transfers between devices: 62.9 us -> none  [body(): lax.psum((part + jnp.dot(heads_two, proj_two, preferred_element_type=jnp....]
    dot_general x24 -> x2, matrix products: 52.9 us -> 11.1 us  [mm(): return jnp.dot(a, b, preferred_element_type=F32)]
    reduce_scatter x1 -> x0, waiting for transfers between devices: 37.8 us -> none  [body(): lax.psum_scatter(partial_value.astype(jnp.float32).astype(jnp.bfloat16),...]
    add x30 -> x0, other arithmetic: 31.4 us -> none  [the longest x16 17.1 us: step(): return (factor[..., None] * state + added, state)]
    rev x14 -> x0, local copies, waits for them, and re-layouts: 29.4 us -> none  [the longest x4 6.87 us: group_local(): vh[:, ::-1]]
  transfers between devices with their start and end apart: 6 -> 0, of which waited for: 4 -> 0; matrix products, arithmetic and copies ran while one was open for 27% -> 0% of each run, Pallas kernels for 0% -> 0%
where the time goes in v1:
time: 171 us; the launch traced here: 170 us
  Pallas kernels  145 us (85%)
  local copies, waits for them, and re-layouts  13.9 us (8%)
  matrix products  11.1 us (6%)
    pallas_call x1, Pallas kernels, body(): call(functools.partial(dispatch_kernel, n, m), shape((n, room, width), BF...  40.3 us
    pallas_call x1, Pallas kernels, body(): call(functools.partial(states_exchange_kernel, n), shape((n, dv + 16, lan...  33.1 us
    pallas_call x1, Pallas kernels, body(): call(functools.partial(return_kernel, n, m), shape((n, room, wide), BF16)...  27.4 us
    pallas_call x1, Pallas kernels, body(): call(functools.partial(settle_kernel, m), [shape((own, width), F32), shap...  19.2 us
    unnamed x57, local copies, waits for them, and re-layouts  13.9 us
    dot_general x2, matrix products, mm(): return jnp.dot(a, b, preferred_element_type=F32)  11.1 us
    pallas_call x1, Pallas kernels, body(): call(functools.partial(mix_kernel, n), shape((rows, width), BF16), [pltpu...  10.9 us
    pallas_call x1, Pallas kernels, body(): call(functools.partial(finish_kernel, m, capacity, experts), shape((own,...  10.6 us

profile of v1, /device:TPU:1, one launch (start us, length us, event | category | flops | bytes accessed | tf_op | source)
XLA Modules:
  0.0 170.1 jit_solution(10576051451343552119)
XLA Ops:
  0.0 1.4 copy-done.4
  1.4 0.9 copy-done.6
  2.3 0.9 copy-done.8
  3.3 0.9 copy-done.10
  4.2 1.0 copy-done.12
  5.3 0.9 copy-done.15
  6.2 2.5 %shard_map.199 = (bf16[2,144,768]{2,1,0:T(8,128)(2,1)S(1)}, f32[2,256,768]{2,1,0:T(8,128)S(1)}) custom-call(bf16[256,256]{1,0:T(8,128)(2,1)S(1)} %copy-done.15, bf16[256,512]{1,0:T(8,128)(2,1)S(1)} %copy-done.6, f32[2,256,256]{2,1,0:T(8,128)S(1)} %copy-done.12, bf16[256,512]{1,0:T(8,128)(2,1)S(1)} %copy-done.8, bf16[256,512]{1,0:T(8,128)(2,1)S(1)} %copy-done.10, ...), custom_call_target="tpu_custom_call" | custom-call | tf_op jit(solution)/shard_map/pallas_call | solution.py:528
  8.8 33.1 %shard_map.200.states = bf16[8,144,768]{2,1,0:T(8,128)(2,1)S(1)} custom-call(bf16[2,144,768]{2,1,0:T(8,128)(2,1)S(1)} %get-tuple-element.9.x), custom_call_target="tpu_custom_call" | custom-call | tf_op jit(solution)/shard_map/pallas_call | solution.py:531
  41.9 1.2 copy-done.1
  43.2 10.9 %shard_map.201.part = bf16[256,2048]{1,0:T(8,128)(2,1)S(1)} custom-call(bf16[8,144,768]{2,1,0:T(8,128)(2,1)} %copy-done.1, f32[2,256,768]{2,1,0:T(8,128)S(1)} %get-tuple-element.10.cum, bf16[256,256]{1,0:T(8,128)(2,1)S(1)} %copy-done.20, bf16[256,256]{1,0:T(8,128)(2,1)S(1)} %copy-done.16, bf16[256,512]{1,0:T(8,128)(2,1)S(1)} %copy-done.7, ...), custom_call_target="tpu_custom_call" | custom-call | tf_op jit(solution)/shard_map/pallas_call | solution.py:538
  54.1 19.2 %shard_map.202 = (f32[64,2048]{1,0:T(8,128)S(1)}, bf16[256,512]{1,0:T(8,128)(2,1)S(1)}) custom-call(bf16[256,2048]{1,0:T(8,128)(2,1)S(1)} %shard_map.201.part, bf16[256,2048]{1,0:T(8,128)(2,1)S(1)} %copy-done.5, f32[1,2048]{1,0:T(1,128)S(1)} %bitcast.27), custom_call_target="tpu_custom_call" | custom-call | tf_op jit(solution)/shard_map/pallas_call | solution.py:547
  73.3 0.9 copy-done.13
  74.2 0.1 copy.23.routes
  74.3 1.0 shard_map.203
  75.3 40.3 %shard_map.204 = bf16[8,96,2048]{2,1,0:T(8,128)(2,1)S(1)} custom-call(bf16[8,96,512]{2,1,0:T(8,128)(2,1)S(1)} %bitcast.26), custom_call_target="tpu_custom_call" | custom-call | tf_op jit(solution)/shard_map/pallas_call | solution.py:558
  115.7 1.6 copy-done.2
  117.3 2.9 %fusion.3 = f32[768,512]{1,0:T(8,128)} fusion(bf16[768,2048]{1,0:T(8,128)(2,1)S(1)} %bitcast.22, bf16[1,2048,512]{2,1,0:T(8,128)(2,1)S(1)} %copy-done.26), kind=kOutput, calls=%fused_computation.4 | convolution fusion | flops 1610612736 | bytes 6815744 | tf_op jit(solution)/shard_map/dot_general | solution.py:30
  120.2 8.1 %convolution_convert_fusion = bf16[768,2048]{1,0:T(8,128)(2,1)} fusion(bf16[1,512,2048]{2,1,0:T(8,128)(2,1)S(1)} %copy-done, f32[768,512]{1,0:T(8,128)} %fusion.3, bf16[768,2048]{1,0:T(8,128)(2,1)} %bitcast.23, bf16[1,2048,512]{2,1,0:T(8,128)(2,1)} %param.40), kind=kOutput, calls=%fused_computation | convolution fusion | flops 3225157632 | bytes 12058624 | tf_op jit(solution)/shard_map/dot_general | solution.py:30
  128.4 1.9 %copy-done.3 = bf16[768,2048]{1,0:T(8,128)(2,1)S(1)} copy-done((bf16[768,2048]{1,0:T(8,128)(2,1)S(1)}, bf16[768,2048]{1,0:T(8,128)(2,1)}, u32[]{:S(2)}) %copy-start.3) | copy-done | bytes 3145752
  130.3 27.4 %shard_map.205 = bf16[8,96,512]{2,1,0:T(8,128)(2,1)S(1)} custom-call(bf16[8,96,2048]{2,1,0:T(8,128)(2,1)S(1)} %bitcast.24), custom_call_target="tpu_custom_call" | custom-call | tf_op jit(solution)/shard_map/pallas_call | solution.py:575
  157.6 0.1 copy.24.affinity
  157.8 1.0 copy-done.14
  158.8 10.6 %shard_map.206 = bf16[64,2048]{1,0:T(8,128)(2,1)S(1)} custom-call(s32[256,2]{1,0:T(8,128)S(1)} %copy.23.routes, f32[256,2]{1,0:T(8,128)S(1)} %copy.24.affinity, bf16[768,512]{1,0:T(8,128)(2,1)S(1)} %bitcast.25, f32[64,2048]{1,0:T(8,128)S(1)} %copy-done.14, f32[1,2048]{1,0:T(1,128)S(1)} %bitcast.28), custom_call_target="tpu_custom_call" | custom-call | tf_op jit(solution)/shard_map/pallas_call | solution.py:585
  169.4 0.7 copy.26
  (43 shorter events, 0.1 us)
Async XLA Ops:
  0.0 120.2 %copy-start = (bf16[1,512,2048]{2,1,0:T(8,128)(2,1)S(1)}, bf16[1,512,2048]{2,1,0:T(8,128)(2,1)}, u32[]{:S(2)}) copy-start(bf16[1,512,2048]{2,1,0:T(8,128)(2,1)} %param.41) | copy-start | bytes 6291460
  0.0 1.4 copy-start.4
  1.4 0.9 copy-start.6
  2.3 0.9 copy-start.8
  4.2 1.0 copy-start.12
  6.2 37.0 %copy-start.7 = (bf16[256,512]{1,0:T(8,128)(2,1)S(1)}, bf16[256,512]{1,0:T(8,128)(2,1)}, u32[]{:S(2)}) copy-start(bf16[256,512]{1,0:T(8,128)(2,1)} %va.3) | copy-start | bytes 786436
  6.2 37.0 %copy-start.9 = (bf16[256,512]{1,0:T(8,128)(2,1)S(1)}, bf16[256,512]{1,0:T(8,128)(2,1)}, u32[]{:S(2)}) copy-start(bf16[256,512]{1,0:T(8,128)(2,1)} %kb.3) | copy-start | bytes 786436
  6.2 37.0 %copy-start.11 = (bf16[256,512]{1,0:T(8,128)(2,1)S(1)}, bf16[256,512]{1,0:T(8,128)(2,1)}, u32[]{:S(2)}) copy-start(bf16[256,512]{1,0:T(8,128)(2,1)} %vb.3) | copy-start | bytes 786436
  6.2 37.0 %copy-start.16 = (bf16[256,256]{1,0:T(8,128)(2,1)S(1)}, bf16[256,256]{1,0:T(8,128)(2,1)}, u32[]{:S(2)}) copy-start(bf16[256,256]{1,0:T(8,128)(2,1)} %ka.3) | copy-start | bytes 393220
  6.2 37.0 %copy-start.17 = (bf16[256,512]{1,0:T(8,128)(2,1)S(1)}, bf16[256,512]{1,0:T(8,128)(2,1)}, u32[]{:S(2)}) copy-start(bf16[256,512]{1,0:T(8,128)(2,1)} %ga.1) | copy-start | bytes 786436
  6.2 37.0 %copy-start.18 = (bf16[256,512]{1,0:T(8,128)(2,1)S(1)}, bf16[256,512]{1,0:T(8,128)(2,1)}, u32[]{:S(2)}) copy-start(bf16[256,512]{1,0:T(8,128)(2,1)} %qb.1) | copy-start | bytes 786436
  6.2 37.0 %copy-start.19 = (bf16[256,512]{1,0:T(8,128)(2,1)S(1)}, bf16[256,512]{1,0:T(8,128)(2,1)}, u32[]{:S(2)}) copy-start(bf16[256,512]{1,0:T(8,128)(2,1)} %gb.1) | copy-start | bytes 786436
  6.2 37.0 %copy-start.20 = (bf16[256,256]{1,0:T(8,128)(2,1)S(1)}, bf16[256,256]{1,0:T(8,128)(2,1)}, u32[]{:S(2)}) copy-start(bf16[256,256]{1,0:T(8,128)(2,1)} %qa.1) | copy-start | bytes 393220
  6.2 37.0 %copy-start.23 = (f32[128]{0:T(128)S(1)}, f32[128]{0:T(128)}, u32[]{:S(2)}) copy-start(f32[128]{0:T(128)} %param.31) | copy-start | bytes 1540
  41.9 1.2 copy-start.1
  43.2 10.9 %copy-start.5 = (bf16[256,2048]{1,0:T(8,128)(2,1)S(1)}, bf16[256,2048]{1,0:T(8,128)(2,1)}, u32[]{:S(2)}) copy-start(bf16[256,2048]{1,0:T(8,128)(2,1)} %stream.1) | copy-start | bytes 3145732
  43.2 10.9 %copy-start.21 = (f32[2048]{0:T(1024)S(1)}, f32[2048]{0:T(1024)}, u32[]{:S(2)}) copy-start(f32[2048]{0:T(1024)} %param.35) | copy-start | bytes 24580
  54.1 20.1 %copy-start.24 = (s32[256,2]{0,1:T(2,128)S(1)}, s32[256,2]{0,1:T(2,128)}, u32[]{:S(2)}) copy-start(s32[256,2]{0,1:T(2,128)} %param.37) | copy-start | bytes 6148
  75.3 42.0 %copy-start.26 = (bf16[1,2048,512]{2,1,0:T(8,128)(2,1)S(1)}, bf16[1,2048,512]{2,1,0:T(8,128)(2,1)}, u32[]{:S(2)}) copy-start(bf16[1,2048,512]{2,1,0:T(8,128)(2,1)} %param.39) | copy-start | bytes 6291460
  115.6 1.6 copy-start.2
  128.4 1.9 %copy-start.3 = (bf16[768,2048]{1,0:T(8,128)(2,1)S(1)}, bf16[768,2048]{1,0:T(8,128)(2,1)}, u32[]{:S(2)}) copy-start(bf16[768,2048]{1,0:T(8,128)(2,1)} %convolution_convert_fusion) | copy-start | bytes 9437188
  130.3 27.4 %copy-start.25 = (f32[256,2]{0,1:T(2,128)S(1)}, f32[256,2]{0,1:T(2,128)}, u32[]{:S(2)}) copy-start(f32[256,2]{0,1:T(2,128)} %param.38) | copy-start | bytes 6148
  130.3 27.5 %copy-start.22 = (f32[2048]{0:T(1024)S(1)}, f32[2048]{0:T(1024)}, u32[]{:S(2)}) copy-start(f32[2048]{0:T(1024)} %param.36) | copy-start | bytes 24580
  157.8 1.0 copy-start.14
  (3 other events, 2.7 us)

commit v2 on v1

--- a/solution.py
+++ b/solution.py
@@ -63,6 +63,15 @@
     return pltpu.make_async_remote_copy(
         src_ref=src, dst_ref=dst, send_sem=send, recv_sem=recv, device_id=peer, device_id_type=MESH
     )
+
+
+def across(me, k, n):
+    place, bit = 0, 1
+    while bit < n:
+        digit = lax.rem(me // bit, 2)
+        place = place + (1 - digit if k & bit else digit) * bit
+        bit *= 2
+    return place
 
 
 def state_kernel(ka, va, da, kb, vb, db, stack, cum):
@@ -98,61 +107,121 @@
                 mm_tn(v[:, h * dv : (h + 1) * dv], weighted[:, h * dk : (h + 1) * dk]).astype(BF16)
                 for h in range(heads)
             ]
-            stack[way, 0:dv, base : base + wide] = (
-                states[0] if heads == 1 else jnp.concatenate(states, axis=1)
-            )
+            states = states[0] if heads == 1 else jnp.concatenate(states, axis=1)
             thigh = tail.astype(BF16).astype(F32)
             row = lax.broadcasted_iota(jnp.int32, (16, wide), 0)
-            stack[way, dv : dv + 16, base : base + wide] = jnp.where(
-                row == 0, thigh, jnp.where(row == 1, tail - thigh, 0.0)
-            ).astype(BF16)
+            fades = jnp.where(row == 0, thigh, jnp.where(row == 1, tail - thigh, 0.0)).astype(BF16)
+            half = dv // 2
+            for i in range(2):
+                stack[i, way, 0:half, base : base + wide] = states[i * half : (i + 1) * half]
+                stack[i, way, half : half + 16, base : base + wide] = fades
         base += wide
 
 
-def states_exchange_kernel(n, x, out, send, recv):
+def spread(total, wide):
+    row = lax.broadcasted_iota(jnp.int32, (16, wide), 0)
+    high = total.astype(BF16).astype(F32)
+    return jnp.where(row == 0, high, jnp.where(row == 1, total - high, 0.0)).astype(BF16)
+
+
+def states_exchange_kernel(n, stack, out, xbox, agg, zbox, outbox, xs, xr, zs, zr, bs, br):
     me = lax.axis_index("sp")
-    greet([{"sp": lax.rem(me + k, n)} for k in range(1, n)])
-    copies = []
-    for k in range(1, n):
-        peer = lax.rem(me + k, n)
-        way = jnp.where(peer < me, 1, 0)
-        copy = remote(x.at[way], out.at[me], send.at[k], recv.at[k], {"sp": peer})
-        copy.start()
-        copies.append(copy)
-    for k in range(1, n):
-        peer = lax.rem(me + k, n)
-        copies[k - 1].wait_send()
-        remote(x.at[0], out.at[lax.rem(me + n - k, n)], send.at[k], recv.at[k], {"sp": peer}).wait_recv()
-
-
-def mix_kernel(
-    n, states, cum, qa, ka, va, ga, qb, kb, vb, gb, gain, pa, pb, out, heads_ref, ahead, behind
-):
-    me = lax.axis_index("sp")
+    side = lax.rem(me, 2)
+    pair = me // 2
+    pairs = n // 2
+    partner = me + 1 - 2 * side
+    half = out.shape[2]
+    lanes = out.shape[3]
+    chunk = 256 if lanes % 256 == 0 else lanes
+    count = lanes // chunk
+
+    def pair_at(j):
+        return lax.rem(pair + j, pairs)
+
+    greet([{"sp": partner}] + [{"sp": pair_at(j) * 2 + side} for j in range(1, pairs)])
+
+    def at(c):
+        return pl.ds(c * chunk, chunk)
+
+    def swap(c):
+        return remote(
+            stack.at[1 - side, :, :, at(c)], xbox.at[:, :, at(c)], xs.at[c], xr.at[c], {"sp": partner}
+        )
+
+    def along(c, j):
+        way = jnp.where(pair_at(j) < pair, 1, 0)
+        return remote(
+            agg.at[way, :, at(c)], zbox.at[pair, :, at(c)], zs.at[c, j], zr.at[c, j],
+            {"sp": pair_at(j) * 2 + side},
+        )
+
+    def back(c):
+        return remote(
+            outbox.at[:, :, at(c)], out.at[:, side, :, at(c)], bs.at[c], br.at[c], {"sp": partner}
+        )
+
+    for c in range(count):
+        swap(c).start()
+    zbox[pair] = jnp.zeros_like(zbox[pair])
+
+    def load(ref, index, c):
+        block = ref[index + (slice(None), at(c))].astype(F32)
+        return block[0:half], block[half : half + 1] + block[half + 1 : half + 2]
+
+    def both(c, way):
+        own, own_fade = load(stack, (side, way), c)
+        other, other_fade = load(xbox, (way,), c)
+        low = side == 0
+        return (
+            jnp.where(low, own, other), jnp.where(low, own_fade, other_fade),
+            jnp.where(low, other, own), jnp.where(low, other_fade, own_fade),
+        )
+
+    for c in range(count):
+        swap(c).wait_recv()
+        s0, t0, s1, t1 = both(c, 0)
+        agg[0, 0:half, at(c)] = (jnp.exp(t1) * s0 + s1).astype(BF16)
+        agg[0, half : half + 16, at(c)] = spread(t0 + t1, chunk)
+        s0, t0, s1, t1 = both(c, 1)
+        agg[1, 0:half, at(c)] = (jnp.exp(t0) * s1 + s0).astype(BF16)
+        agg[1, half : half + 16, at(c)] = spread(t0 + t1, chunk)
+        for j in range(1, pairs):
+            along(c, j).start()
+    for c in range(count):
+        for j in range(1, pairs):
+            along(c, j).wait_recv()
+        ahead = jnp.zeros((half, chunk), F32)
+        behind = jnp.zeros((half, chunk), F32)
+        for s in range(pairs):
+            state, fade = load(zbox, (s,), c)
+            ahead = jnp.where(s < pair, jnp.exp(fade) * ahead + state, ahead)
+        for s in reversed(range(pairs)):
+            state, fade = load(zbox, (s,), c)
+            behind = jnp.where(s > pair, jnp.exp(fade) * behind + state, behind)
+        low = side == 0
+        s0, t0, _, _ = both(c, 0)
+        next_ahead = jnp.exp(t0) * ahead + s0
+        _, _, s1, t1 = both(c, 1)
+        next_behind = jnp.exp(t1) * behind + s1
+        outbox[0, :, at(c)] = jnp.where(low, next_ahead, ahead).astype(BF16)
+        outbox[1, :, at(c)] = jnp.where(low, behind, next_behind).astype(BF16)
+        back(c).start()
+        out[0, side, :, at(c)] = jnp.where(low, ahead, next_ahead).astype(BF16)
+        out[1, side, :, at(c)] = jnp.where(low, next_behind, behind).astype(BF16)
+    for c in range(count):
+        swap(c).wait_send()
+        for j in range(1, pairs):
+            along(c, j).wait_send()
+        back(c).wait_send()
+        remote(
+            outbox.at[:, :, at(c)], out.at[:, 1 - side, :, at(c)], bs.at[c], br.at[c], {"sp": partner}
+        ).wait_recv()
+
+
+def mix_kernel(states, cum, qa, ka, va, ga, qb, kb, vb, gb, gain, pa, pb, out, heads_ref):
     rows = qa.shape[0]
     count = rows // BLK
-    dv = ahead.shape[0]
-    ahead[...] = jnp.zeros_like(ahead)
-    behind[...] = jnp.zeros_like(behind)
-
-    def join(total, source):
-        fade = states[source, dv : dv + 1, :].astype(F32) + states[source, dv + 1 : dv + 2, :].astype(F32)
-        total[...] = jnp.exp(fade) * total[...] + states[source, 0:dv, :].astype(F32)
-
-    def one(s, carry):
-        @pl.when(s < me)
-        def _():
-            join(ahead, s)
-
-        back = n - 1 - s
-
-        @pl.when(back > me)
-        def _():
-            join(behind, back)
-
-        return carry
-
-    lax.fori_loop(0, n, one, 0)
+    dv = gain.shape[1]
     ii = lax.broadcasted_iota(jnp.int32, (BLK, BLK), 0)
     jj = lax.broadcasted_iota(jnp.int32, (BLK, BLK), 1)
     base = 0
@@ -163,8 +232,8 @@
             lanes = slice(base + h * dk, base + (h + 1) * dk)
             own = slice(h * dk, (h + 1) * dk)
             vown = slice(h * dv, (h + 1) * dv)
-            forward = ahead[:, lanes]
-            backward = behind[:, lanes]
+            forward = jnp.concatenate([states[0, i, :, lanes] for i in range(2)], axis=0).astype(F32)
+            backward = jnp.concatenate([states[1, i, :, lanes] for i in range(2)], axis=0).astype(F32)
             mixed = [None] * count
             readers = [None] * count
             growth = [None] * count
@@ -213,10 +282,15 @@
         ).astype(BF16)
 
 
-def settle_kernel(n, part, stream, gain, settled, columns, inbox, outbox, send, recv, send2, recv2):
+def settle_kernel(
+    n, part, stream, gain, settled, columns, inbox, mid, midbox, outbox, cs, cr, ys, yr, send2, recv2
+):
     me = lax.axis_index("tp")
     own = part.shape[0] // n
     wide = part.shape[1] // n
+    core = lax.rem(me, 2)
+    line = me // 2
+    lines = n // 2
     greet([{"tp": lax.rem(me + k, n)} for k in range(1, n)])
 
     def rows_of(i):
@@ -225,16 +299,31 @@
     def cols_of(i):
         return pl.ds(pl.multiple_of(i * wide, wide), wide)
 
-    copies = []
-    for k in range(1, n):
-        peer = lax.rem(me + k, n)
-        copy = remote(part.at[rows_of(peer), :], inbox.at[k], send.at[k], recv.at[k], {"tp": peer})
-        copy.start()
-        copies.append(copy)
-    total = part[rows_of(me), :].astype(F32)
-    for k in range(1, n):
-        copies[k - 1].wait_recv()
-        total = total + inbox[k].astype(F32)
+    def line_at(j):
+        return lax.rem(line + j, lines)
+
+    def to_core(j):
+        i = line_at(j) * 2 + 1 - core
+        return remote(
+            part.at[rows_of(i), :], inbox.at[j], cs.at[j], cr.at[j], {"tp": me + 1 - 2 * core}
+        )
+
+    def to_line(j):
+        return remote(mid.at[j], midbox.at[j], ys.at[j], yr.at[j], {"tp": line_at(j) * 2 + core})
+
+    for j in reversed(range(lines)):
+        to_core(j).start()
+    for j in reversed(range(lines)):
+        to_core(j).wait_recv()
+        mine = part[rows_of(line_at(j) * 2 + core), :].astype(F32) + inbox[j].astype(F32)
+        if j > 0:
+            mid[j] = mine.astype(BF16)
+            to_line(j).start()
+        else:
+            total = mine
+    for j in range(1, lines):
+        to_line(j).wait_recv()
+        total = total + midbox[j].astype(F32)
     total = total.astype(BF16).astype(F32)
     value = layer_norm(stream[rows_of(me), :].astype(F32) + total, gain[...])
     settled[...] = value
@@ -250,11 +339,14 @@
     columns[rows_of(me), :] = outbox[:, cols_of(me)]
     for k in range(1, n):
         source = lax.rem(me + n - k, n)
-        copies[k - 1].wait_send()
         second[k - 1].wait_send()
         remote(
             outbox.at[:, cols_of(source)], columns.at[rows_of(source), :], send2.at[k], recv2.at[k], {"tp": source}
         ).wait_recv()
+    for j in range(lines):
+        to_core(j).wait_send()
+        if j > 0:
+            to_line(j).wait_send()
 
 
 def slots_of(routes, capacity, experts):
@@ -305,7 +397,7 @@
     )
 
     def cross(k):
-        peer = lax.rem(me + k, n)
+        peer = across(me, k, n)
         return remote(x.at[peer], out.at[me, :, cols_of(my)], ss.at[k], sr.at[k], {"sp": peer})
 
     for k in range(1, n):
@@ -326,7 +418,7 @@
         return remote(block(s, i), block(s, i), fs.at[k, j], fr.at[k, j], {"tp": partner})
 
     def source(k):
-        return lax.rem(me + n - k, n)
+        return across(me, k, n)
 
     def hand_on(k, s):
         for j in range(1, lines):
@@ -382,7 +474,7 @@
     )
 
     def place(k):
-        return lax.rem(me + k + 1, n)
+        return across(me, n - 1 - k, n)
 
     def to_core(k, j):
         i = line_at(j) * 2 + 1 - core
@@ -433,7 +525,7 @@
                 to_line(k, j).wait_send()
         if k < n - 1:
             cross(k).wait_send()
-            s = lax.rem(me + 2 * n - k - 1, n)
+            s = place(k)
             remote(last.at[k], out.at[s], ss.at[k], sr.at[k], {"sp": s}).wait_recv()
 
 
@@ -525,29 +617,36 @@
     capacity = 3 * rows * top // (2 * experts)
     room = local_experts * capacity
 
+    half = dv // 2
     stack, cum = call(
-        state_kernel, [shape((2, dv + 16, lanes), BF16), shape((2, rows, lanes), F32)], [], 6
+        state_kernel, [shape((2, 2, half + 16, lanes), BF16), shape((2, rows, lanes), F32)], [], 6
     )(key_one, value_one, decay_one, key_two, value_two, decay_two)
+    chunks = max(1, lanes // 256)
     states = call(
         functools.partial(states_exchange_kernel, n),
-        shape((n, dv + 16, lanes), BF16),
-        [DMA((n,)), DMA((n,))],
+        shape((2, 2, half, lanes), BF16),
+        [
+            pltpu.VMEM((2, half + 16, lanes), BF16),
+            pltpu.VMEM((2, half + 16, lanes), BF16),
+            pltpu.VMEM((n // 2, half + 16, lanes), BF16),
+            pltpu.VMEM((2, half, lanes), BF16),
+            DMA((chunks,)), DMA((chunks,)), DMA((chunks, n // 2)), DMA((chunks, n // 2)),
+            DMA((chunks,)), DMA((chunks,)),
+        ],
         1,
         1,
     )(stack)
-    part = call(
-        functools.partial(mix_kernel, n),
-        shape((rows, width), BF16),
-        [pltpu.VMEM((rows, values), BF16), pltpu.VMEM((dv, lanes), F32), pltpu.VMEM((dv, lanes), F32)],
-        13,
-    )(
+    part = call(mix_kernel, shape((rows, width), BF16), [pltpu.VMEM((rows, values), BF16)], 13)(
         states, cum, query_one, key_one, value_one, gate_one, query_two, key_two, value_two, gate_two,
         head_gain.reshape(1, -1), proj_one, proj_two,
     )
     settled, columns = call(
         functools.partial(settle_kernel, m),
         [shape((own, width), F32), shape((rows, wide), BF16)],
-        [pltpu.VMEM((m, own, width), BF16), pltpu.VMEM((own, width), BF16)] + [DMA((m,))] * 4,
+        [pltpu.VMEM((m // 2, own, width), BF16)] * 3
+        + [pltpu.VMEM((own, width), BF16)]
+        + [DMA((m // 2,))] * 4
+        + [DMA((m,))] * 2,
         3,
         2,
     )(part, stream, gain_mix.reshape(1, -1))

time: 171 us -> 138 us (0.81)
  Pallas kernels: 145 us -> 114 us
    pallas_call x3, Pallas kernels: 46.5 us -> 31.5 us  [the longest x1 19.1 us: body(): call(functools.partial(states_exchange_kernel, n), shape((2, 2, half, lan...]
    pallas_call x1, Pallas kernels: 40.3 us -> 28.9 us  [body(): call(functools.partial(dispatch_kernel, n, m), shape((n, room, width), BF...]
    pallas_call x1, Pallas kernels: 10.6 us -> 7.91 us  [body(): call(functools.partial(finish_kernel, m, capacity, experts), shape((own,...]
    unnamed x57 -> x53, local copies, waits for them, and re-layouts: 13.9 us -> 12.6 us
where the time goes in v2:
time: 138 us
  Pallas kernels  114 us (83%)
  local copies, waits for them, and re-layouts  12.6 us (9%)
  matrix products  11.1 us (8%)
    pallas_call x1, Pallas kernels, body(): call(functools.partial(dispatch_kernel, n, m), shape((n, room, width), BF...  28.9 us
    pallas_call x1, Pallas kernels, body(): call(functools.partial(return_kernel, n, m), shape((n, room, wide), BF16)...  26.1 us
    pallas_call x1, Pallas kernels, body(): call(functools.partial(states_exchange_kernel, n), shape((2, 2, half, lan...  19.1 us
    pallas_call x1, Pallas kernels, body(): call(functools.partial(settle_kernel, m), [shape((own, width), F32), shap...  18.3 us
    unnamed x53, local copies, waits for them, and re-layouts  12.6 us
    dot_general x2, matrix products, mm(): return jnp.dot(a, b, preferred_element_type=F32)  11.1 us
    pallas_call x1, Pallas kernels, body(): call(mix_kernel, shape((rows, width), BF16), [pltpu.VMEM((rows, values),...  9.83 us
    pallas_call x1, Pallas kernels, body(): call(functools.partial(finish_kernel, m, capacity, experts), shape((own,...  7.91 us

profile of v2, /device:TPU:1, one launch (start us, length us, event | category | flops | bytes accessed | tf_op | source)
XLA Modules:
  0.0 137.6 jit_solution(16282343256616177120)
XLA Ops:
  0.0 1.1 copy-done.3
  1.1 0.9 copy-done.5
  2.1 0.9 copy-done.6
  3.0 1.2 copy-done.8
  4.2 0.9 copy-done.10
  5.1 1.0 copy-done.12
  6.2 2.5 %shard_map.199 = (bf16[2,2,80,768]{3,2,1,0:T(8,128)(2,1)S(1)}, f32[2,256,768]{2,1,0:T(8,128)S(1)}) custom-call(bf16[256,256]{1,0:T(8,128)(2,1)S(1)} %copy-done.10, bf16[256,512]{1,0:T(8,128)(2,1)S(1)} %copy-done.3, f32[2,256,256]{2,1,0:T(8,128)S(1)} %copy-done.12, bf16[256,512]{1,0:T(8,128)(2,1)S(1)} %copy-done.5, bf16[256,512]{1,0:T(8,128)(2,1)S(1)} %copy-done.6, ...), custom_call_target="tpu_custom_call" | custom-call | tf_op jit(solution)/shard_map/pallas_call | solution.py:621
  8.8 19.1 %shard_map.200.states = bf16[2,2,64,768]{3,2,1,0:T(8,128)(2,1)S(1)} custom-call(bf16[2,2,80,768]{3,2,1,0:T(8,128)(2,1)S(1)} %get-tuple-element.9.stack), custom_call_target="tpu_custom_call" | custom-call | tf_op jit(solution)/shard_map/pallas_call | solution.py:625
  27.9 0.0 copy-start.9
  28.0 9.8 %shard_map.201.part = bf16[256,2048]{1,0:T(8,128)(2,1)S(1)} custom-call(bf16[2,2,64,768]{3,2,1,0:T(8,128)(2,1)S(1)} %shard_map.200.states, f32[2,256,768]{2,1,0:T(8,128)S(1)} %get-tuple-element.10.cum, bf16[256,256]{1,0:T(8,128)(2,1)S(1)} %copy-done.18, bf16[256,256]{1,0:T(8,128)(2,1)S(1)} %copy-done.11, bf16[256,512]{1,0:T(8,128)(2,1)S(1)} %copy-done.4, ...), custom_call_target="tpu_custom_call" | custom-call | tf_op jit(solution)/shard_map/pallas_call | solution.py:639
  37.8 18.3 %shard_map.202 = (f32[64,2048]{1,0:T(8,128)S(1)}, bf16[256,512]{1,0:T(8,128)(2,1)S(1)}) custom-call(bf16[256,2048]{1,0:T(8,128)(2,1)S(1)} %shard_map.201.part, bf16[256,2048]{1,0:T(8,128)(2,1)S(1)} %copy-done.9, f32[1,2048]{1,0:T(1,128)S(1)} %bitcast.27), custom_call_target="tpu_custom_call" | custom-call | tf_op jit(solution)/shard_map/pallas_call | solution.py:643
  56.2 0.9 copy-done.13
  57.1 0.1 copy.23.routes
  57.2 1.0 shard_map.203
  58.2 28.9 %shard_map.204 = bf16[8,96,2048]{2,1,0:T(8,128)(2,1)S(1)} custom-call(bf16[8,96,512]{2,1,0:T(8,128)(2,1)S(1)} %bitcast.26), custom_call_target="tpu_custom_call" | custom-call | tf_op jit(solution)/shard_map/pallas_call | solution.py:657
  87.1 1.6 %copy-done.1 = bf16[8,96,2048]{2,1,0:T(8,128)(2,1)} copy-done((bf16[8,96,2048]{2,1,0:T(8,128)(2,1)}, bf16[8,96,2048]{2,1,0:T(8,128)(2,1)S(1)}, u32[]{:S(2)}) %copy-start.1) | copy-done | bytes 3145752
  88.7 2.9 %fusion.3 = f32[768,512]{1,0:T(8,128)} fusion(bf16[768,2048]{1,0:T(8,128)(2,1)S(1)} %bitcast.22, bf16[1,2048,512]{2,1,0:T(8,128)(2,1)S(1)} %copy-done.24), kind=kOutput, calls=%fused_computation.4 | convolution fusion | flops 1610612736 | bytes 6815744 | tf_op jit(solution)/shard_map/dot_general | solution.py:30
  91.6 8.1 %convolution_convert_fusion = bf16[768,2048]{1,0:T(8,128)(2,1)} fusion(bf16[1,512,2048]{2,1,0:T(8,128)(2,1)S(1)} %copy-done, f32[768,512]{1,0:T(8,128)} %fusion.3, bf16[768,2048]{1,0:T(8,128)(2,1)} %bitcast.23, bf16[1,2048,512]{2,1,0:T(8,128)(2,1)} %param.40), kind=kOutput, calls=%fused_computation | convolution fusion | flops 3225157632 | bytes 12058624 | tf_op jit(solution)/shard_map/dot_general | solution.py:30
  99.8 1.9 %copy-done.2 = bf16[768,2048]{1,0:T(8,128)(2,1)S(1)} copy-done((bf16[768,2048]{1,0:T(8,128)(2,1)S(1)}, bf16[768,2048]{1,0:T(8,128)(2,1)}, u32[]{:S(2)}) %copy-start.2) | copy-done | bytes 3145752
  101.7 26.1 %shard_map.205 = bf16[8,96,512]{2,1,0:T(8,128)(2,1)S(1)} custom-call(bf16[8,96,2048]{2,1,0:T(8,128)(2,1)S(1)} %bitcast.24), custom_call_target="tpu_custom_call" | custom-call | tf_op jit(solution)/shard_map/pallas_call | solution.py:674
  127.8 0.1 copy.24.affinity
  127.9 1.0 copy-done.14
  129.0 7.9 %shard_map.206 = bf16[64,2048]{1,0:T(8,128)(2,1)S(1)} custom-call(s32[256,2]{1,0:T(8,128)S(1)} %copy.23.routes, f32[256,2]{1,0:T(8,128)S(1)} %copy.24.affinity, bf16[768,512]{1,0:T(8,128)(2,1)S(1)} %bitcast.25, f32[64,2048]{1,0:T(8,128)S(1)} %copy-done.14, f32[1,2048]{1,0:T(1,128)S(1)} %bitcast.28), custom_call_target="tpu_custom_call" | custom-call | tf_op jit(solution)/shard_map/pallas_call | solution.py:684
  136.9 0.7 copy.26
  (39 shorter events, 0.1 us)
Async XLA Ops:
  0.0 91.6 %copy-start = (bf16[1,512,2048]{2,1,0:T(8,128)(2,1)S(1)}, bf16[1,512,2048]{2,1,0:T(8,128)(2,1)}, u32[]{:S(2)}) copy-start(bf16[1,512,2048]{2,1,0:T(8,128)(2,1)} %param.41) | copy-start | bytes 6291460
  0.0 1.1 copy-start.3
  1.1 0.9 copy-start.5
  2.1 0.9 copy-start.6
  3.0 1.2 copy-start.8
  4.2 0.9 copy-start.10
  5.1 1.0 copy-start.12
  6.2 21.7 %copy-start.4 = (bf16[256,512]{1,0:T(8,128)(2,1)S(1)}, bf16[256,512]{1,0:T(8,128)(2,1)}, u32[]{:S(2)}) copy-start(bf16[256,512]{1,0:T(8,128)(2,1)} %va.3) | copy-start | bytes 786436
  6.2 21.7 %copy-start.7 = (bf16[256,512]{1,0:T(8,128)(2,1)S(1)}, bf16[256,512]{1,0:T(8,128)(2,1)}, u32[]{:S(2)}) copy-start(bf16[256,512]{1,0:T(8,128)(2,1)} %vb.3) | copy-start | bytes 786436
  6.2 21.7 %copy-start.11 = (bf16[256,256]{1,0:T(8,128)(2,1)S(1)}, bf16[256,256]{1,0:T(8,128)(2,1)}, u32[]{:S(2)}) copy-start(bf16[256,256]{1,0:T(8,128)(2,1)} %ka.3) | copy-start | bytes 393220
  6.2 21.7 %copy-start.15 = (bf16[256,512]{1,0:T(8,128)(2,1)S(1)}, bf16[256,512]{1,0:T(8,128)(2,1)}, u32[]{:S(2)}) copy-start(bf16[256,512]{1,0:T(8,128)(2,1)} %ga.1) | copy-start | bytes 786436
  6.2 21.7 %copy-start.16 = (bf16[256,512]{1,0:T(8,128)(2,1)S(1)}, bf16[256,512]{1,0:T(8,128)(2,1)}, u32[]{:S(2)}) copy-start(bf16[256,512]{1,0:T(8,128)(2,1)} %qb.1) | copy-start | bytes 786436
  6.2 21.7 %copy-start.17 = (bf16[256,512]{1,0:T(8,128)(2,1)S(1)}, bf16[256,512]{1,0:T(8,128)(2,1)}, u32[]{:S(2)}) copy-start(bf16[256,512]{1,0:T(8,128)(2,1)} %gb.1) | copy-start | bytes 786436
  6.2 21.7 %copy-start.18 = (bf16[256,256]{1,0:T(8,128)(2,1)S(1)}, bf16[256,256]{1,0:T(8,128)(2,1)}, u32[]{:S(2)}) copy-start(bf16[256,256]{1,0:T(8,128)(2,1)} %qa.1) | copy-start | bytes 393220
  6.2 21.7 %copy-start.21 = (f32[128]{0:T(128)S(1)}, f32[128]{0:T(128)}, u32[]{:S(2)}) copy-start(f32[128]{0:T(128)} %param.31) | copy-start | bytes 1540
  27.9 9.9 %copy-start.9 = (bf16[256,2048]{1,0:T(8,128)(2,1)S(1)}, bf16[256,2048]{1,0:T(8,128)(2,1)}, u32[]{:S(2)}) copy-start(bf16[256,2048]{1,0:T(8,128)(2,1)} %stream.1) | copy-start | bytes 3145732
  28.0 9.9 %copy-start.19 = (f32[2048]{0:T(1024)S(1)}, f32[2048]{0:T(1024)}, u32[]{:S(2)}) copy-start(f32[2048]{0:T(1024)} %param.35) | copy-start | bytes 24580
  37.8 19.3 %copy-start.22 = (s32[256,2]{0,1:T(2,128)S(1)}, s32[256,2]{0,1:T(2,128)}, u32[]{:S(2)}) copy-start(s32[256,2]{0,1:T(2,128)} %param.37) | copy-start | bytes 6148
  58.2 30.5 %copy-start.24 = (bf16[1,2048,512]{2,1,0:T(8,128)(2,1)S(1)}, bf16[1,2048,512]{2,1,0:T(8,128)(2,1)}, u32[]{:S(2)}) copy-start(bf16[1,2048,512]{2,1,0:T(8,128)(2,1)} %param.39) | copy-start | bytes 6291460
  87.1 1.6 %copy-start.1 = (bf16[8,96,2048]{2,1,0:T(8,128)(2,1)}, bf16[8,96,2048]{2,1,0:T(8,128)(2,1)S(1)}, u32[]{:S(2)}) copy-start(bf16[8,96,2048]{2,1,0:T(8,128)(2,1)S(1)} %shard_map.204) | copy-start | bytes 9437188
  99.8 1.9 %copy-start.2 = (bf16[768,2048]{1,0:T(8,128)(2,1)S(1)}, bf16[768,2048]{1,0:T(8,128)(2,1)}, u32[]{:S(2)}) copy-start(bf16[768,2048]{1,0:T(8,128)(2,1)} %convolution_convert_fusion) | copy-start | bytes 9437188
  101.7 26.1 %copy-start.23 = (f32[256,2]{0,1:T(2,128)S(1)}, f32[256,2]{0,1:T(2,128)}, u32[]{:S(2)}) copy-start(f32[256,2]{0,1:T(2,128)} %param.38) | copy-start | bytes 6148
  101.7 26.2 %copy-start.20 = (f32[2048]{0:T(1024)S(1)}, f32[2048]{0:T(1024)}, u32[]{:S(2)}) copy-start(f32[2048]{0:T(1024)} %param.36) | copy-start | bytes 24580
  127.9 1.0 copy-start.14
  (1 other events, 0.9 us)

commit v3 on v2

--- a/solution.py
+++ b/solution.py
@@ -74,7 +74,14 @@
     return place
 
 
-def state_kernel(ka, va, da, kb, vb, db, stack, cum):
+def state_kernel(*refs):
+    held, stack, cum, local, sems = refs[:6], refs[6], refs[7], refs[8:14], refs[14]
+    loads = [pltpu.make_async_copy(a, b, sems.at[i]) for i, (a, b) in enumerate(zip(held, local))]
+    for load in loads:
+        load.start()
+    for load in loads:
+        load.wait()
+    ka, va, da, kb, vb, db = local
     rows = ka.shape[0]
     count = rows // BLK
     ii = lax.broadcasted_iota(jnp.int32, (rows, rows), 0)
@@ -618,9 +625,15 @@
     room = local_experts * capacity
 
     half = dv // 2
-    stack, cum = call(
-        state_kernel, [shape((2, 2, half + 16, lanes), BF16), shape((2, rows, lanes), F32)], [], 6
-    )(key_one, value_one, decay_one, key_two, value_two, decay_two)
+    inputs = (key_one, value_one, decay_one, key_two, value_two, decay_two)
+    stack, cum = pl.pallas_call(
+        state_kernel,
+        out_shape=[shape((2, 2, half + 16, lanes), BF16), shape((2, rows, lanes), F32)],
+        in_specs=[pl.BlockSpec(memory_space=pltpu.HBM)] * len(inputs),
+        out_specs=[VMEM] * 2,
+        scratch_shapes=[pltpu.VMEM(a.shape, a.dtype) for a in inputs] + [DMA((len(inputs),))],
+        compiler_params=pltpu.CompilerParams(vmem_limit_bytes=60 * 1024 * 1024),
+    )(*inputs)
     chunks = max(1, lanes // 256)
     states = call(
         functools.partial(states_exchange_kernel, n),

time: 138 us -> 137 us (level)
  local copies, waits for them, and re-layouts: 12.6 us -> 8.85 us
  Pallas kernels: 114 us -> 117 us
    unnamed x53 -> x47, local copies, waits for them, and re-layouts: 12.6 us -> 8.85 us
    pallas_call x1, Pallas kernels: 2.52 us -> 5.47 us  [body(): pl.pallas_call(state_kernel, out_shape=[shape((2, 2, half + 16, lanes), B...]
where the time goes in v3:
time: 137 us
  Pallas kernels  117 us (85%)
  matrix products  11.1 us (8%)
  local copies, waits for them, and re-layouts  8.85 us (6%)
    pallas_call x1, Pallas kernels, body(): call(functools.partial(dispatch_kernel, n, m), shape((n, room, width), BF...  28.9 us
    pallas_call x1, Pallas kernels, body(): call(functools.partial(return_kernel, n, m), shape((n, room, wide), BF16)...  26.1 us
    pallas_call x1, Pallas kernels, body(): call(functools.partial(states_exchange_kernel, n), shape((2, 2, half, lan...  19.1 us
    pallas_call x1, Pallas kernels, body(): call(functools.partial(settle_kernel, m), [shape((own, width), F32), shap...  18.4 us
    dot_general x2, matrix products, mm(): return jnp.dot(a, b, preferred_element_type=F32)  11.1 us
    pallas_call x1, Pallas kernels, body(): call(mix_kernel, shape((rows, width), BF16), [pltpu.VMEM((rows, values),...  9.85 us
    unnamed x47, local copies, waits for them, and re-layouts  8.85 us
    pallas_call x1, Pallas kernels, body(): call(functools.partial(finish_kernel, m, capacity, experts), shape((own,...  7.93 us

profile of v3, /device:TPU:1, one launch (start us, length us, event | category | flops | bytes accessed | tf_op | source)
XLA Modules:
  0.0 136.8 jit_solution(17825711194452922513)
XLA Ops:
  0.1 5.5 %shard_map.199 = (bf16[2,2,80,768]{3,2,1,0:T(8,128)(2,1)}, f32[2,256,768]{2,1,0:T(8,128)}) custom-call(bf16[256,256]{1,0:T(8,128)(2,1)} %ka.1, bf16[256,512]{1,0:T(8,128)(2,1)} %va.1, f32[2,256,256]{2,1,0:T(8,128)} %refs_2_.1, bf16[256,512]{1,0:T(8,128)(2,1)} %kb.1, bf16[256,512]{1,0:T(8,128)(2,1)} %vb.1, f32[2,256,512]{2,1,0:T(8,128)} %refs_5_.1), custom_call_target="tpu_custom_call" | custom-call | tf_op jit(solution)/shard_map/pallas_call | solution.py:629
  5.6 1.0 copy-done.11
  6.6 19.1 %shard_map.200.states = bf16[2,2,64,768]{3,2,1,0:T(8,128)(2,1)S(1)} custom-call(bf16[2,2,80,768]{3,2,1,0:T(8,128)(2,1)S(1)} %copy-done.11), custom_call_target="tpu_custom_call" | custom-call | tf_op jit(solution)/shard_map/pallas_call | solution.py:638
  25.8 1.4 %copy-done.3 = f32[2,256,768]{2,1,0:T(8,128)S(1)} copy-done((f32[2,256,768]{2,1,0:T(8,128)S(1)}, f32[2,256,768]{2,1,0:T(8,128)}, u32[]{:S(2)}) %copy-start.3) | copy-done | bytes 1572888
  27.2 9.9 %shard_map.201.part = bf16[256,2048]{1,0:T(8,128)(2,1)S(1)} custom-call(bf16[2,2,64,768]{3,2,1,0:T(8,128)(2,1)S(1)} %shard_map.200.states, f32[2,256,768]{2,1,0:T(8,128)S(1)} %copy-done.3, bf16[256,256]{1,0:T(8,128)(2,1)S(1)} %copy-done.15, bf16[256,256]{1,0:T(8,128)(2,1)S(1)} %copy-done.8, bf16[256,512]{1,0:T(8,128)(2,1)S(1)} %copy-done.4, ...), custom_call_target="tpu_custom_call" | custom-call | tf_op jit(solution)/shard_map/pallas_call | solution.py:652
  37.0 0.0 copy-start.19
  37.1 18.4 %shard_map.202 = (f32[64,2048]{1,0:T(8,128)S(1)}, bf16[256,512]{1,0:T(8,128)(2,1)S(1)}) custom-call(bf16[256,2048]{1,0:T(8,128)(2,1)S(1)} %shard_map.201.part, bf16[256,2048]{1,0:T(8,128)(2,1)S(1)} %copy-done.7, f32[1,2048]{1,0:T(1,128)S(1)} %bitcast.27), custom_call_target="tpu_custom_call" | custom-call | tf_op jit(solution)/shard_map/pallas_call | solution.py:656
  55.4 0.8 copy-done.9
  56.3 0.0 copy-done.19
  56.3 0.1 copy.23.routes
  56.4 1.0 shard_map.203
  57.4 0.0 copy-start.21
  57.4 28.9 %shard_map.204 = bf16[8,96,2048]{2,1,0:T(8,128)(2,1)S(1)} custom-call(bf16[8,96,512]{2,1,0:T(8,128)(2,1)S(1)} %bitcast.26), custom_call_target="tpu_custom_call" | custom-call | tf_op jit(solution)/shard_map/pallas_call | solution.py:670
  86.3 1.6 %copy-done.1 = bf16[8,96,2048]{2,1,0:T(8,128)(2,1)} copy-done((bf16[8,96,2048]{2,1,0:T(8,128)(2,1)}, bf16[8,96,2048]{2,1,0:T(8,128)(2,1)S(1)}, u32[]{:S(2)}) %copy-start.1) | copy-done | bytes 3145752
  87.9 2.9 %fusion.3 = f32[768,512]{1,0:T(8,128)} fusion(bf16[768,2048]{1,0:T(8,128)(2,1)S(1)} %bitcast.22, bf16[1,2048,512]{2,1,0:T(8,128)(2,1)S(1)} %copy-done.21), kind=kOutput, calls=%fused_computation.4 | convolution fusion | flops 1610612736 | bytes 6815744 | tf_op jit(solution)/shard_map/dot_general | solution.py:30
  90.9 8.1 %convolution_convert_fusion = bf16[768,2048]{1,0:T(8,128)(2,1)} fusion(bf16[1,512,2048]{2,1,0:T(8,128)(2,1)S(1)} %copy-done, f32[768,512]{1,0:T(8,128)} %fusion.3, bf16[768,2048]{1,0:T(8,128)(2,1)} %bitcast.23, bf16[1,2048,512]{2,1,0:T(8,128)(2,1)} %param.40), kind=kOutput, calls=%fused_computation | convolution fusion | flops 3225157632 | bytes 12058624 | tf_op jit(solution)/shard_map/dot_general | solution.py:30
  99.0 1.9 %copy-done.2 = bf16[768,2048]{1,0:T(8,128)(2,1)S(1)} copy-done((bf16[768,2048]{1,0:T(8,128)(2,1)S(1)}, bf16[768,2048]{1,0:T(8,128)(2,1)}, u32[]{:S(2)}) %copy-start.2) | copy-done | bytes 3145752
  100.9 26.1 %shard_map.205 = bf16[8,96,512]{2,1,0:T(8,128)(2,1)S(1)} custom-call(bf16[8,96,2048]{2,1,0:T(8,128)(2,1)S(1)} %bitcast.24), custom_call_target="tpu_custom_call" | custom-call | tf_op jit(solution)/shard_map/pallas_call | solution.py:687
  127.0 0.1 copy.24.affinity
  127.1 0.0 copy-done.17
  127.1 0.0 copy-start.10
  127.2 1.0 copy-done.10
  128.2 7.9 %shard_map.206 = bf16[64,2048]{1,0:T(8,128)(2,1)S(1)} custom-call(s32[256,2]{1,0:T(8,128)S(1)} %copy.23.routes, f32[256,2]{1,0:T(8,128)S(1)} %copy.24.affinity, bf16[768,512]{1,0:T(8,128)(2,1)S(1)} %bitcast.25, f32[64,2048]{1,0:T(8,128)S(1)} %copy-done.10, f32[1,2048]{1,0:T(1,128)S(1)} %bitcast.28), custom_call_target="tpu_custom_call" | custom-call | tf_op jit(solution)/shard_map/pallas_call | solution.py:697
  136.1 0.7 copy.26
  (33 shorter events, 0.1 us)
Async XLA Ops:
  0.0 90.9 %copy-start = (bf16[1,512,2048]{2,1,0:T(8,128)(2,1)S(1)}, bf16[1,512,2048]{2,1,0:T(8,128)(2,1)}, u32[]{:S(2)}) copy-start(bf16[1,512,2048]{2,1,0:T(8,128)(2,1)} %param.41) | copy-start | bytes 6291460
  0.0 25.7 %copy-start.8 = (bf16[256,256]{1,0:T(8,128)(2,1)S(1)}, bf16[256,256]{1,0:T(8,128)(2,1)}, u32[]{:S(2)}) copy-start(bf16[256,256]{1,0:T(8,128)(2,1)} %ka.1) | copy-start | bytes 393220
  0.0 25.7 %copy-start.4 = (bf16[256,512]{1,0:T(8,128)(2,1)S(1)}, bf16[256,512]{1,0:T(8,128)(2,1)}, u32[]{:S(2)}) copy-start(bf16[256,512]{1,0:T(8,128)(2,1)} %va.1) | copy-start | bytes 786436
  0.0 25.7 %copy-start.5 = (bf16[256,512]{1,0:T(8,128)(2,1)S(1)}, bf16[256,512]{1,0:T(8,128)(2,1)}, u32[]{:S(2)}) copy-start(bf16[256,512]{1,0:T(8,128)(2,1)} %kb.1) | copy-start | bytes 786436
  0.0 25.7 %copy-start.6 = (bf16[256,512]{1,0:T(8,128)(2,1)S(1)}, bf16[256,512]{1,0:T(8,128)(2,1)}, u32[]{:S(2)}) copy-start(bf16[256,512]{1,0:T(8,128)(2,1)} %vb.1) | copy-start | bytes 786436
  0.0 25.7 %copy-start.18 = (f32[128]{0:T(128)S(1)}, f32[128]{0:T(128)}, u32[]{:S(2)}) copy-start(f32[128]{0:T(128)} %param.31) | copy-start | bytes 1540
  0.0 25.7 %copy-start.15 = (bf16[256,256]{1,0:T(8,128)(2,1)S(1)}, bf16[256,256]{1,0:T(8,128)(2,1)}, u32[]{:S(2)}) copy-start(bf16[256,256]{1,0:T(8,128)(2,1)} %qa.1) | copy-start | bytes 393220
  0.1 25.7 %copy-start.12 = (bf16[256,512]{1,0:T(8,128)(2,1)S(1)}, bf16[256,512]{1,0:T(8,128)(2,1)}, u32[]{:S(2)}) copy-start(bf16[256,512]{1,0:T(8,128)(2,1)} %ga.1) | copy-start | bytes 786436
  0.1 25.7 %copy-start.13 = (bf16[256,512]{1,0:T(8,128)(2,1)S(1)}, bf16[256,512]{1,0:T(8,128)(2,1)}, u32[]{:S(2)}) copy-start(bf16[256,512]{1,0:T(8,128)(2,1)} %qb.1) | copy-start | bytes 786436
  0.1 25.7 %copy-start.14 = (bf16[256,512]{1,0:T(8,128)(2,1)S(1)}, bf16[256,512]{1,0:T(8,128)(2,1)}, u32[]{:S(2)}) copy-start(bf16[256,512]{1,0:T(8,128)(2,1)} %gb.1) | copy-start | bytes 786436
  5.6 1.0 copy-start.11
  25.8 1.4 %copy-start.3 = (f32[2,256,768]{2,1,0:T(8,128)S(1)}, f32[2,256,768]{2,1,0:T(8,128)}, u32[]{:S(2)}) copy-start(f32[2,256,768]{2,1,0:T(8,128)} %get-tuple-element.10.cum) | copy-start | bytes 4718596
  27.2 9.9 %copy-start.7 = (bf16[256,2048]{1,0:T(8,128)(2,1)S(1)}, bf16[256,2048]{1,0:T(8,128)(2,1)}, u32[]{:S(2)}) copy-start(bf16[256,2048]{1,0:T(8,128)(2,1)} %stream.1) | copy-start | bytes 3145732
  27.2 9.9 %copy-start.16 = (f32[2048]{0:T(1024)S(1)}, f32[2048]{0:T(1024)}, u32[]{:S(2)}) copy-start(f32[2048]{0:T(1024)} %param.35) | copy-start | bytes 24580
  37.0 19.2 %copy-start.19 = (s32[256,2]{0,1:T(2,128)S(1)}, s32[256,2]{0,1:T(2,128)}, u32[]{:S(2)}) copy-start(s32[256,2]{0,1:T(2,128)} %param.37) | copy-start | bytes 6148
  55.4 0.8 copy-start.9
  57.4 30.5 %copy-start.21 = (bf16[1,2048,512]{2,1,0:T(8,128)(2,1)S(1)}, bf16[1,2048,512]{2,1,0:T(8,128)(2,1)}, u32[]{:S(2)}) copy-start(bf16[1,2048,512]{2,1,0:T(8,128)(2,1)} %param.39) | copy-start | bytes 6291460
  86.3 1.6 %copy-start.1 = (bf16[8,96,2048]{2,1,0:T(8,128)(2,1)}, bf16[8,96,2048]{2,1,0:T(8,128)(2,1)S(1)}, u32[]{:S(2)}) copy-start(bf16[8,96,2048]{2,1,0:T(8,128)(2,1)S(1)} %shard_map.204) | copy-start | bytes 9437188
  99.0 1.9 %copy-start.2 = (bf16[768,2048]{1,0:T(8,128)(2,1)S(1)}, bf16[768,2048]{1,0:T(8,128)(2,1)}, u32[]{:S(2)}) copy-start(bf16[768,2048]{1,0:T(8,128)(2,1)} %convolution_convert_fusion) | copy-start | bytes 9437188
  100.9 26.1 %copy-start.20 = (f32[256,2]{0,1:T(2,128)S(1)}, f32[256,2]{0,1:T(2,128)}, u32[]{:S(2)}) copy-start(f32[256,2]{0,1:T(2,128)} %param.38) | copy-start | bytes 6148
  100.9 26.2 %copy-start.17 = (f32[2048]{0:T(1024)S(1)}, f32[2048]{0:T(1024)}, u32[]{:S(2)}) copy-start(f32[2048]{0:T(1024)} %param.36) | copy-start | bytes 24580
  127.1 1.0 copy-start.10
